TPU v7x, 32 devices: a whole 2x2x4 slice. The times are simulated.
32 devices in a mesh: ep: 16 (over z, x, core), tp: 2 (over y).
Axes of the slice: x: 2, y: 2, z: 4, core: 2. Of those that a mesh axis runs over, the one named last changes fastest.
Arguments:
- tokens: bfloat16 [256, 2048], P('ep', 'tp'), may hold values from -6 to 6
- state: bfloat16 [256, 32, 4096], P('ep', 'tp'), may hold values from -6 to 6
- mix_gain: float32 [2048], P('tp'), may hold values from 0.1 to 1.9
- w_recept: bfloat16 [2048, 2048], P('tp', 'ep'), may hold values from -0.125 to 0.125
- w_key: bfloat16 [2048, 2048], P('tp', 'ep'), may hold values from -0.125 to 0.125
- w_value: bfloat16 [2048, 2048], P('tp', 'ep'), may hold values from -0.125 to 0.125
- w_decay: bfloat16 [2048, 2048], P('tp', 'ep'), may hold values from -0.125 to 0.125
- w_rate: bfloat16 [2048, 2048], P('tp', 'ep'), may hold values from -0.125 to 0.125
- decay_base: float32 [2048], P('tp'), may hold values from -4 to 2
- rate_base: float32 [2048], P('tp'), may hold values from -2 to 2
- head_gain: float32 [2048], P('tp'), may hold values from 0.1 to 1.9
- w_out: bfloat16 [2048, 2048], P('tp', 'ep'), may hold values from -0.125 to 0.125
- moe_gain: float32 [2048], replicated, may hold values from 0.1 to 1.9
- routes: int32 [256, 6], P('ep'), may hold values from 0 to 15, all different within a row; in each aligned block of 16 rows (0 to 15, 16 to 31, ...) at most 12 rows name the same one
- route_weight: float32 [256, 6], P('ep'), may hold values from 0.1 to 1
- expert_gate: bfloat16 [16, 2048, 512], P('ep', None, 'tp'), may hold values from -0.125 to 0.125
- expert_up: bfloat16 [16, 2048, 512], P('ep', None, 'tp'), may hold values from -0.125 to 0.125
- expert_down: bfloat16 [16, 512, 2048], P('ep', 'tp'), may hold values from -0.25 to 0.25
- shared_gate: bfloat16 [2048, 512], P(None, 'tp'), may hold values from -0.125 to 0.125
- shared_up: bfloat16 [2048, 512], P(None, 'tp'), may hold values from -0.125 to 0.125
- shared_down: bfloat16 [512, 2048], P('tp'), may hold values from -0.25 to 0.25
Outputs:
- layer_out: bfloat16 [256, 2048], P('ep', 'tp')
Inputs may be any that keep to these rules, and one draw needn't show every extreme that they name: `routes`: each row names 6 different experts. Within the rows of one device (aligned blocks of 16 rows) no expert is named by more than 12 rows, a bound that some block reaches.
All inputs are finite; a program needn't handle non-finite values.
Results may differ from a plain program's by a relative error of at most 0.024.
Values may be sent and summed in bfloat16 or wider, within the bound.
No kernel may reach another device: no remote copies, remote signals or barrier semaphores. Data moves between devices by JAX's collectives and lax.ppermute only.
A program may use at most 64 MiB of HBM per device.

v0:
```python
import jax
import jax.numpy as jnp
from jax import lax
from jax.sharding import PartitionSpec as P

HEAD = 64


RMS_EPS = 1e-06
GN_EPS = 0.00064
KEY_EPS = 1e-06
ROUTED_SCALE = 2.5


def for_sending(array):
    return jax.tree.map(lambda a: a.astype(jnp.bfloat16) if a.dtype == jnp.float32 else a, array)


def mixer_rows(state_rows, projected, decay_base, rate_base, head_gain):
    seq_count = projected.shape[0]
    head_count = projected.shape[2] // HEAD

    def per_head(column):
        return projected[:, column, :].reshape(seq_count, head_count, HEAD)

    receptance = per_head(0)
    key_vec = per_head(1)
    value_vec = per_head(2)
    decay_pre = (projected[:, 3, :] + decay_base).reshape(seq_count, head_count, HEAD)
    rate_pre = (projected[:, 4, :] + rate_base).reshape(seq_count, head_count, HEAD)
    decay_rate = jnp.exp(-jnp.exp(-jax.nn.softplus(-decay_pre) - 0.5))
    in_rate = jax.nn.sigmoid(rate_pre)
    unit_key = key_vec * lax.rsqrt(jnp.sum(key_vec * key_vec, axis=-1, keepdims=True) + KEY_EPS)
    carried = state_rows.astype(jnp.float32).reshape(seq_count, head_count, HEAD, HEAD)
    removed = jnp.einsum("nhvk,nhk->nhv", carried, unit_key)
    updated = (
        carried * decay_rate[:, :, None, :]
        - removed[:, :, :, None] * (unit_key * in_rate)[:, :, None, :]
        + value_vec[:, :, :, None] * (key_vec * in_rate)[:, :, None, :]
    )
    readout = jnp.einsum("nhvk,nhk->nhv", updated, receptance)
    centre = jnp.mean(readout, axis=-1, keepdims=True)
    spread = jnp.mean(jnp.square(readout - centre), axis=-1, keepdims=True)
    normed = (readout - centre) * lax.rsqrt(spread + GN_EPS)
    return (normed.reshape(seq_count, head_count * HEAD) * head_gain).astype(jnp.bfloat16)


def quarter_sums(partial_value):
    return jax.tree.map(
        lambda part: part.astype(jnp.float32),
        lax.psum_scatter(for_sending(partial_value), "tp", scatter_dimension=2, tiled=True),
    )


def project_split(part_rows, weight_cols):
    inner_len = weight_cols.shape[0]
    role_count = weight_cols.shape[1]
    col_width = weight_cols.shape[2]
    flat_weight = weight_cols.reshape(inner_len, role_count * col_width)
    block_rows = lax.all_gather(part_rows, "ep", axis=0, tiled=True)
    product = jnp.dot(block_rows, flat_weight, preferred_element_type=jnp.float32)
    gathered = product.astype(jnp.bfloat16).reshape(block_rows.shape[0], role_count, col_width)
    owned = lax.all_to_all(gathered, "ep", split_axis=0, concat_axis=2, tiled=True)
    return quarter_sums(owned.astype(jnp.float32))


def body(
    tokens,
    state,
    mix_gain,
    w_recept,
    w_key,
    w_value,
    w_decay,
    w_rate,
    decay_base,
    rate_base,
    head_gain,
    w_out,
    moe_gain,
    routes,
    route_weight,
    expert_gate,
    expert_up,
    expert_down,
    shared_gate,
    shared_up,
    shared_down,
):
    seq_count = tokens.shape[0]
    quarter = tokens.shape[1]
    width_all = quarter * lax.axis_size("tp")
    ep_count = lax.axis_size("ep")
    topk_count = routes.shape[1]
    capacity = min(seq_count, max(2, 2 * seq_count * topk_count // ep_count))
    tokens32 = tokens.astype(jnp.float32)
    square_sum = lax.psum(jnp.sum(tokens32 * tokens32, axis=1), "tp")
    factor = lax.rsqrt(square_sum / width_all + RMS_EPS)
    normed = (tokens32 * factor[:, None] * mix_gain).astype(jnp.bfloat16)
    stacked = jnp.stack((w_recept, w_key, w_value, w_decay, w_rate), axis=1)
    projected = project_split(normed, stacked)
    mixed = mixer_rows(state, projected, decay_base, rate_base, head_gain)
    attended = project_split(mixed, w_out[:, None, :])[:, 0, :]
    resid = (tokens32 + attended).astype(jnp.bfloat16)
    full_resid = lax.all_gather(resid, "tp", axis=1, tiled=True).astype(jnp.float32)
    moe_factor = lax.rsqrt(jnp.mean(full_resid * full_resid, axis=1, keepdims=True) + RMS_EPS)
    normed_two = (full_resid * moe_factor * moe_gain).astype(jnp.bfloat16)
    shared_hidden = (
        jax.nn.silu(jnp.dot(normed_two, shared_gate, preferred_element_type=jnp.float32))
        * jnp.dot(normed_two, shared_up, preferred_element_type=jnp.float32)
    ).astype(jnp.bfloat16)
    shared_part = jnp.dot(shared_hidden, shared_down, preferred_element_type=jnp.float32)
    entry_count = seq_count * topk_count
    flat_routes = routes.reshape(entry_count)
    position = jnp.arange(entry_count, dtype=jnp.int32)
    earlier = (flat_routes[:, None] == flat_routes[None, :]) & (
        position[None, :] < position[:, None]
    )
    rank_in = jnp.sum(earlier.astype(jnp.int32), axis=1)
    local_slot = flat_routes * capacity + rank_in
    slot_count = ep_count * capacity
    slot_ids = jnp.arange(slot_count, dtype=jnp.int32)
    matches = (slot_ids[:, None] == local_slot[None, :]).astype(jnp.float32)
    dispatch_map = jnp.sum(matches.reshape(slot_count, seq_count, topk_count), axis=2).astype(
        jnp.bfloat16
    )
    outgoing = jnp.dot(dispatch_map, normed_two, preferred_element_type=jnp.float32)
    outgoing = outgoing.astype(jnp.bfloat16).reshape(ep_count, capacity, width_all)
    arrived = lax.all_to_all(outgoing, "ep", split_axis=0, concat_axis=0, tiled=True)
    expert_in = arrived.reshape(slot_count, width_all)
    hidden = (
        jax.nn.silu(jnp.dot(expert_in, expert_gate[0], preferred_element_type=jnp.float32))
        * jnp.dot(expert_in, expert_up[0], preferred_element_type=jnp.float32)
    ).astype(jnp.bfloat16)
    expert_part = jnp.dot(hidden, expert_down[0], preferred_element_type=jnp.float32)
    routed_sum, shared_sum = quarter_sums((expert_part[:, None, :], shared_part[:, None, :]))
    expert_out = routed_sum[:, 0, :].astype(jnp.bfloat16).reshape(ep_count, capacity, quarter)
    came_back = lax.all_to_all(expert_out, "ep", split_axis=0, concat_axis=0, tiled=True).reshape(
        slot_count, quarter
    )
    picked = (
        jnp.take(came_back, local_slot, axis=0)
        .astype(jnp.float32)
        .reshape(seq_count, topk_count, quarter)
    )
    share = route_weight / jnp.sum(route_weight, axis=1, keepdims=True) * ROUTED_SCALE
    routed = jnp.sum(share[:, :, None] * picked, axis=1)
    return (resid.astype(jnp.float32) + routed + shared_sum[:, 0, :]).astype(jnp.bfloat16)


def solution(mesh):
    placed = (
        P("ep", "tp"),
        P("ep", "tp", None),
        P("tp"),
        P("tp", "ep"),
        P("tp", "ep"),
        P("tp", "ep"),
        P("tp", "ep"),
        P("tp", "ep"),
        P("tp"),
        P("tp"),
        P("tp"),
        P("tp", "ep"),
        P(),
        P("ep", None),
        P("ep", None),
        P("ep", None, "tp"),
        P("ep", None, "tp"),
        P("ep", "tp", None),
        P(None, "tp"),
        P(None, "tp"),
        P("tp", None),
    )
    return jax.shard_map(body, mesh=mesh, in_specs=placed, out_specs=P("ep", "tp"), check_vma=False)
```

profile of v0, /device:TPU:0, one launch (start us, length us, event | category | flops | bytes accessed | tf_op | source)
XLA Modules:
  0.0 221.4 jit_solution(4564653830152176430)
XLA Ops:
  6.6 1.2 copy.77
  10.2 5.9 %psum.7 = f32[16]{0:T(128)S(1)} all-reduce(f32[16]{0:T(128)S(1)} %fusion.37), channel_id=1, replica_groups=mesh['ep'=16,'tp'=2] {'tp'}, use_global_device_ids=true, to_apply=%region_1.0 | all-reduce | flops 16 | bytes 128 | tf_op jit(solution)/shard_map/psum | solution.py:97
  16.2 23.7 %all_gather.9 = bf16[256,1024]{1,0:T(8,128)(2,1)S(1)} all-gather(bf16[16,1024]{1,0:T(8,128)(2,1)S(1)} %fusion.39), channel_id=1, replica_groups=mesh['ep'=16,'tp'=2] {'ep'}, dimensions={0}, use_global_device_ids=true | all-gather | bytes 557056 | tf_op jit(solution)/shard_map/all_gather | solution.py:60
  42.9 1.9 convolution_convert_fusion.3
  46.0 17.9 %all_to_all.46 = bf16[256,5,128]{2,1,0:T(8,128)(2,1)S(1)} all-to-all(bf16[256,5,128]{2,1,0:T(8,128)(2,1)} %copy.83), channel_id=1, replica_groups=mesh['ep'=16,'tp'=2] {'ep'}, dimensions={0} | all-to-all | bytes 655360 | tf_op jit(solution)/shard_map/all_to_all | solution.py:63
  65.3 5.5 %reshape.193 = bf16[16,16,64,64]{3,2,1,0:T(8,128)(2,1)} reshape(bf16[16,16,4096]{2,1,0:T(8,128)(2,1)S(1)} %copy-done.2) | data formatting | bytes 4194304 | tf_op jit(solution)/shard_map/reshape | solution.py:34
  70.8 6.4 %reduce-scatter.5.cloned.1.call-done = bf16[16,5,1024]{2,0,1:T(8,128)(2,1)} async-done(((bf16[16,5,2048]{2,0,1:T(8,128)(2,1)}), bf16[16,5,1024]{2,0,1:T(8,128)(2,1)}) %reduce-scatter.5.cloned.1.call-update) | async-done | bytes 163856 | tf_op jit(solution)/shard_map/reduce_scatter | solution.py:51
  79.6 4.6 %fusion.63 = f32[16,16,1,64]{3,2,1,0:T(1,128)S(1)} fusion(f32[16,16,64,1]{2,3,1,0:T(1,128)S(1)} %bitcast.94, bf16[16,16,64,64]{3,2,1,0:T(8,128)(2,1)} %reshape.193), kind=kOutput, calls=%fused_computation.100 | convolution fusion | flops 2097152 | bytes 2228224 | tf_op jit(solution)/shard_map/nhvk,nhk->nhv/dot_general | solution.py:35
  84.2 5.8 %fusion = f32[16,16,1,64]{3,2,1,0:T(1,128)S(1)} fusion(bf16[16,16,64,1]{2,3,1,0:T(2,128)(2,1)S(1)} %reshape.218, bf16[16,16,64,64]{3,2,1,0:T(8,128)(2,1)S(1)} %copy-done.1, f32[16,16,64]{2,1,0:T(8,128)S(1)} %get-tuple-element.9, f32[16,16,64]{2,1,0:T(8,128)S(1)} %mul.188, f32[16,16,64]{2,1,0:T(8,128)S(1)} %get-tuple-element.7, ...), kind=kOutput, calls=%fused_computation.1 | convolution fusion | flops 8388608 | bytes 2523136 | tf_op jit(solution)/shard_map/nhvk,nhk->nhv/dot_general | solution.py:41
  90.6 22.9 %all_gather.10 = bf16[256,1024]{1,0:T(8,128)(2,1)S(1)} all-gather(bf16[16,1024]{1,0:T(8,128)(2,1)S(1)} %multiply_convert_fusion), channel_id=1, replica_groups=mesh['ep'=16,'tp'=2] {'ep'}, dimensions={0}, use_global_device_ids=true | all-gather | bytes 557056 | tf_op jit(solution)/shard_map/all_gather | solution.py:60
  115.6 3.5 %all-to-all-start.1 = ((bf16[16,2,1024]{2,1,0:T(2,128)(2,1)}), bf16[16,2,1024]{2,1,0:T(2,128)(2,1)S(1)}, u32[]{:S(2)}, u32[]{:S(2)}) async-start(bf16[16,2,1024]{2,1,0:T(2,128)(2,1)} %reshape.223), calls=%async_computation.2 | async-start | bytes 131072 | tf_op jit(solution)/shard_map/all_to_all | solution.py:63
  119.6 6.4 %all-to-all-done.1 = bf16[16,2,1024]{2,1,0:T(2,128)(2,1)S(1)} async-done(((bf16[16,2,1024]{2,1,0:T(2,128)(2,1)}), bf16[16,2,1024]{2,1,0:T(2,128)(2,1)S(1)}, u32[]{:S(2)}, u32[]{:S(2)}) %all-to-all-start.1) | async-done | bytes 65568 | tf_op jit(solution)/shard_map/all_to_all | solution.py:63
  127.0 6.3 %reduce-scatter.7.cloned.1.call-done = bf16[16,1,1024]{2,0,1:T(8,128)(2,1)} async-done(((bf16[16,1,2048]{2,0,1:T(8,128)(2,1)}), bf16[16,1,1024]{2,0,1:T(8,128)(2,1)}) %reduce-scatter.7.cloned.1.call-update) | async-done | bytes 32784 | tf_op jit(solution)/shard_map/reduce_scatter | solution.py:51
  134.0 4.6 %all_gather.11 = bf16[16,2048]{1,0:T(8,128)(2,1)S(1)} all-gather(bf16[16,1024]{1,0:T(8,128)(2,1)S(1)} %fusion.40), channel_id=1, replica_groups=mesh['ep'=16,'tp'=2] {'tp'}, dimensions={1}, use_global_device_ids=true | all-gather | bytes 98304 | tf_op jit(solution)/shard_map/all_gather | solution.py:105
  139.4 30.1 %all_to_all.47 = bf16[16,12,2048]{2,1,0:T(8,128)(2,1)S(1)} all-to-all(bf16[16,12,2048]{2,1,0:T(8,128)(2,1)S(1)} %reshape.200), channel_id=1, replica_groups=mesh['ep'=16,'tp'=2] {'ep'}, dimensions={0} | all-to-all | bytes 1572864 | tf_op jit(solution)/shard_map/all_to_all | solution.py:129
  169.6 1.7 fusion.19
  171.3 1.9 fusion.12
  173.5 16.9 %reduce-scatter.9.cloned.1.call-done = bf16[192,1,1024]{2,0,1:T(8,128)(2,1)} async-done(((bf16[192,1,2048]{2,0,1:T(8,128)(2,1)}), bf16[192,1,1024]{2,0,1:T(8,128)(2,1)}) %reduce-scatter.9.cloned.1.call-update) | async-done | bytes 393232 | tf_op jit(solution)/shard_map/reduce_scatter | solution.py:51
  190.4 1.9 convert_element_type.98
  192.3 5.6 %all-to-all-start.3 = ((bf16[16,12,1024]{2,1,0:T(8,128)(2,1)}), bf16[16,12,1024]{2,1,0:T(8,128)(2,1)S(1)}, u32[]{:S(2)}, u32[]{:S(2)}) async-start(bf16[16,12,1024]{2,1,0:T(8,128)(2,1)} %convert_element_type.98), calls=%async_computation.6 | async-start | bytes 1048576 | tf_op jit(solution)/shard_map/all_to_all | solution.py:138
  198.0 1.5 fusion.58
  199.5 2.6 %fusion.13 = bf16[16,1,2048]{2,0,1:T(8,128)(2,1)} fusion(bf16[256,2048]{1,0:T(8,128)(2,1)S(1)} %copy-done.3, bf16[2048,256]{1,0:T(8,128)(2,1)} %param.40, f32[16,256]{1,0:T(8,128)S(1)} %fusion.58, bf16[16,2048]{1,0:T(8,128)(2,1)S(1)} %all_gather.11, f32[2048]{0:T(1024)S(1)} %copy-done.10, f32[16]{0:T(128)S(1)} %add_rsqrt_fusion.2), kind=kOutput, calls=%fused_computation.17 | convolution fusion | flops 33742848 | bytes 2252864 | tf_op jit(solution)/shard_map/dot_general | solution.py:112
  202.2 10.0 %all-to-all-done.3 = bf16[16,12,1024]{2,1,0:T(8,128)(2,1)S(1)} async-done(((bf16[16,12,1024]{2,1,0:T(8,128)(2,1)}), bf16[16,12,1024]{2,1,0:T(8,128)(2,1)S(1)}, u32[]{:S(2)}, u32[]{:S(2)}) %all-to-all-start.3) | async-done | bytes 393248 | tf_op jit(solution)/shard_map/all_to_all | solution.py:138
  213.5 1.4 fusion.41
  (109 shorter events, 17.6 us)
Async XLA Ops:
  6.5 164.8 %copy-start = (bf16[1,256,2048]{2,1,0:T(8,128)(2,1)S(1)}, bf16[1,256,2048]{2,1,0:T(8,128)(2,1)}, u32[]{:S(2)}) copy-start(bf16[1,256,2048]{2,1,0:T(8,128)(2,1)} %param.38) | copy-start | bytes 3145732
  6.5 3.1 %copy-start.6 = (bf16[1024,128]{1,0:T(8,128)(2,1)S(1)}, bf16[1024,128]{1,0:T(8,128)(2,1)}, u32[]{:S(2)}) copy-start(bf16[1024,128]{1,0:T(8,128)(2,1)} %param.26) | copy-start | bytes 786436
  6.5 3.2 %copy-start.7 = (bf16[1024,128]{1,0:T(8,128)(2,1)S(1)}, bf16[1024,128]{1,0:T(8,128)(2,1)}, u32[]{:S(2)}) copy-start(bf16[1024,128]{1,0:T(8,128)(2,1)} %param.27) | copy-start | bytes 786436
  6.5 3.4 %copy-start.8 = (bf16[1024,128]{1,0:T(8,128)(2,1)S(1)}, bf16[1024,128]{1,0:T(8,128)(2,1)}, u32[]{:S(2)}) copy-start(bf16[1024,128]{1,0:T(8,128)(2,1)} %param.28) | copy-start | bytes 786436
  6.5 3.6 %copy-start.5 = (bf16[16,1024]{1,0:T(8,128)(2,1)S(1)}, bf16[16,1024]{1,0:T(8,128)(2,1)}, u32[]{:S(2)}) copy-start(bf16[16,1024]{1,0:T(8,128)(2,1)} %param.21) | copy-start | bytes 98308
  6.5 9.6 %copy-start.12 = (f32[1024]{0:T(1024)S(1)}, f32[1024]{0:T(1024)}, u32[]{:S(2)}) copy-start(f32[1024]{0:T(1024)} %param.23) | copy-start | bytes 12292
  6.6 70.7 %reduce-scatter.5.cloned.1.call-start = ((), (), s32[]{:S(2)}) async-start(), calls=%async_computation.8 | async-start | bytes 491520 | tf_op jit(solution)/shard_map/reduce_scatter | solution.py:51
  46.0 19.1 %copy-start.13 = (f32[1024]{0:T(1024)S(1)}, f32[1024]{0:T(1024)}, u32[]{:S(2)}) copy-start(f32[1024]{0:T(1024)} %param.29) | copy-start | bytes 12292
  46.0 19.2 %copy-start.14 = (f32[1024]{0:T(1024)S(1)}, f32[1024]{0:T(1024)}, u32[]{:S(2)}) copy-start(f32[1024]{0:T(1024)} %param.30) | copy-start | bytes 12292
  46.0 19.2 %copy-start.2 = (bf16[16,16,4096]{2,1,0:T(8,128)(2,1)S(1)}, bf16[16,16,4096]{2,1,0:T(8,128)(2,1)}, u32[]{:S(2)}) copy-start(bf16[16,16,4096]{2,1,0:T(8,128)(2,1)} %param.22) | copy-start | bytes 6291460
  79.6 4.6 %copy-start.1 = (bf16[16,16,64,64]{3,2,1,0:T(8,128)(2,1)S(1)}, bf16[16,16,64,64]{3,2,1,0:T(8,128)(2,1)}, u32[]{:S(2)}) copy-start(bf16[16,16,64,64]{3,2,1,0:T(8,128)(2,1)} %reshape.193) | copy-start | bytes 6291460
  84.2 6.4 %copy-start.15 = (f32[1024]{0:T(1024)S(1)}, f32[1024]{0:T(1024)}, u32[]{:S(2)}) copy-start(f32[1024]{0:T(1024)} %param.31) | copy-start | bytes 12292
  84.2 29.3 %copy-start.9 = (bf16[1024,128]{1,0:T(8,128)(2,1)S(1)}, bf16[1024,128]{1,0:T(8,128)(2,1)}, u32[]{:S(2)}) copy-start(bf16[1024,128]{1,0:T(8,128)(2,1)} %param.32) | copy-start | bytes 786436
  90.0 29.2 %copy-start.16 = (s32[16,6]{0,1:T(8,128)S(1)}, s32[16,6]{0,1:T(8,128)}, u32[]{:S(2)}) copy-start(s32[16,6]{0,1:T(8,128)} %param.34) | copy-start | bytes 1156
  90.5 48.3 %copy-start.10 = (f32[2048]{0:T(1024)S(1)}, f32[2048]{0:T(1024)}, u32[]{:S(2)}) copy-start(f32[2048]{0:T(1024)} %param.33) | copy-start | bytes 24580
  115.6 10.4 %all-to-all-start.1 = ((bf16[16,2,1024]{2,1,0:T(2,128)(2,1)}), bf16[16,2,1024]{2,1,0:T(2,128)(2,1)S(1)}, u32[]{:S(2)}, u32[]{:S(2)}) async-start(bf16[16,2,1024]{2,1,0:T(2,128)(2,1)} %reshape.223), calls=%async_computation.2 | async-start | bytes 131072 | tf_op jit(solution)/shard_map/all_to_all | solution.py:63
  119.1 14.1 %reduce-scatter.7.cloned.1.call-start = ((), (), s32[]{:S(2)}) async-start(), calls=%async_computation.9 | async-start | bytes 98304 | tf_op jit(solution)/shard_map/reduce_scatter | solution.py:51
  126.7 63.7 %reduce-scatter.9.cloned.1.call-start = ((), (), s32[]{:S(2)}) async-start(), calls=%async_computation.10 | async-start | bytes 1179648 | tf_op jit(solution)/shard_map/reduce_scatter | solution.py:51
  169.6 1.7 copy-start.4
  171.3 2.1 copy-start.11
  173.3 26.2 %copy-start.3 = (bf16[256,2048]{1,0:T(8,128)(2,1)S(1)}, bf16[256,2048]{1,0:T(8,128)(2,1)}, u32[]{:S(2)}) copy-start(bf16[256,2048]{1,0:T(8,128)(2,1)} %param.41) | copy-start | bytes 3145732
  192.3 19.9 %all-to-all-start.3 = ((bf16[16,12,1024]{2,1,0:T(8,128)(2,1)}), bf16[16,12,1024]{2,1,0:T(8,128)(2,1)S(1)}, u32[]{:S(2)}, u32[]{:S(2)}) async-start(bf16[16,12,1024]{2,1,0:T(8,128)(2,1)} %convert_element_type.98), calls=%async_computation.6 | async-start | bytes 1048576 | tf_op jit(solution)/shard_map/all_to_all | solution.py:138
  197.9 15.6 %reduce-scatter.11.cloned.1.call-start = ((), (), s32[]{:S(2)}) async-start(), calls=%async_computation.11 | async-start | bytes 98304 | tf_op jit(solution)/shard_map/reduce_scatter | solution.py:51
Sparse Core Ops, SparseCore 0:
  65.2 11.9 reduce-scatter.4
  126.8 6.3 reduce-scatter.6
  173.4 16.9 reduce-scatter.8
  202.3 10.3 reduce-scatter.10
where the time goes:
time: 222 us; the launch traced here: 221 us
  blocking collectives  105 us (47%)
  waiting for transfers between devices  46.1 us (21%)
  local copies, waits for them, and re-layouts  22.1 us (10%)
  matrix products  20.8 us (9%)
  between operations  13.6 us (6%)
  starting transfers between devices  9.27 us (4%)
  other arithmetic  4.52 us (2%)
    all_gather x2, blocking collectives, project_split(): block_rows = lax.all_gather(part_rows, 'ep', axis=0, tiled=True)  46.6 us
    all_to_all x1, blocking collectives, body(): lax.all_to_all(outgoing, 'ep', split_axis=0, concat_axis=0, tiled=True)  30.1 us
    reduce_scatter x4, waiting for transfers between devices, quarter_sums(): lax.psum_scatter(for_sending(partial_value), 'tp', scatter_dimension=2, t...  29.7 us
    all_to_all x1, blocking collectives, project_split(): lax.all_to_all(gathered, 'ep', split_axis=0, concat_axis=2, tiled=True)  17.9 us
    all_to_all x1, waiting for transfers between devices, body(): lax.all_to_all(expert_out, 'ep', split_axis=0, concat_axis=0, tiled=True)  10 us
    unnamed x47, local copies, waits for them, and re-layouts  6.46 us
    all_to_all x1, waiting for transfers between devices, project_split(): lax.all_to_all(gathered, 'ep', split_axis=0, concat_axis=2, tiled=True)  6.36 us
    psum x1, blocking collectives, body(): square_sum = lax.psum(jnp.sum(tokens32 * tokens32, axis=1), 'tp')  5.89 us
  transfers between devices with their start and end apart: 6, of which 5 were waited for; matrix products, arithmetic and copies ran while one was open for 5% of the time, Pallas kernels for 0%

commit v1 on v0

v1 whole, which is shorter than its diff:
```python
import jax
import jax.numpy as jnp
from jax import lax
from jax.sharding import Mesh, PartitionSpec as P

HEAD = 64


RMS_EPS = 1e-06
GN_EPS = 0.00064
KEY_EPS = 1e-06
ROUTED_SCALE = 2.5

F32 = jnp.float32
BF16 = jnp.bfloat16


def core_swap(array):
    return lax.ppermute(array, "core", [(0, 1), (1, 0)])


def spread_rows(rows):
    chips = lax.axis_size("chip")
    copies = jnp.broadcast_to(rows[None], (chips,) + rows.shape)
    return lax.all_to_all(copies, "chip", 0, 0, tiled=True)


def both(own, other):
    core = lax.axis_index("core")
    first = jnp.where(core == 0, own, other)
    second = jnp.where(core == 0, other, own)
    return first, second


def body(
    tokens,
    state,
    mix_gain,
    w_recept,
    w_key,
    w_value,
    w_decay,
    w_rate,
    decay_base,
    rate_base,
    head_gain,
    w_out,
    moe_gain,
    routes,
    route_weight,
    expert_gate,
    expert_up,
    expert_down,
    shared_gate,
    shared_up,
    shared_down,
):
    chips = lax.axis_size("chip")
    tp = lax.axis_size("tp")
    chip = lax.axis_index("chip")
    core = lax.axis_index("core")
    shard = lax.axis_index("tp")
    seqs, part = tokens.shape
    width = part * tp
    cols = w_out.shape[1]
    wide = 2 * cols
    experts = 2 * chips
    topk = routes.shape[1]
    chips_tp = chips // tp

    weights = (w_recept, w_key, w_value, w_decay, w_rate)
    roles = len(weights)
    own_w = jnp.concatenate(weights, axis=1)
    other_w = core_swap(own_w)
    other_out = core_swap(w_out)
    other_gate = core_swap(expert_gate[0])
    other_up = core_swap(expert_up[0])
    other_down = core_swap(expert_down[0])

    rows = spread_rows(tokens).reshape(chips * seqs, part)
    scaled = (rows.astype(F32) * mix_gain).astype(BF16)
    own_p = jnp.dot(scaled, own_w, preferred_element_type=F32).astype(BF16)
    other_p = jnp.dot(scaled, other_w, preferred_element_type=F32).astype(BF16)
    first, second = both(own_p, other_p)
    first = first.reshape(chips, seqs, roles, cols)
    second = second.reshape(chips, seqs, roles, cols)
    sent = jnp.concatenate((first, second), axis=3)
    got = lax.all_to_all(sent, "chip", 0, 0, tiled=True).reshape(
        tp, chips_tp, seqs, roles, wide
    )
    square_sum = jnp.sum(jnp.square(tokens.astype(F32)), axis=1)
    square_tile = jnp.broadcast_to(square_sum[:, None], (seqs, 128))
    total = lax.dynamic_index_in_dim(got, shard, 0, keepdims=False).astype(F32)
    square_total = square_tile
    for step in range(1, tp):
        order = [(i, (i + step) % tp) for i in range(tp)]
        block = lax.dynamic_index_in_dim(got, (shard + step) % tp, 0, keepdims=False)
        total = total + lax.ppermute(block, "tp", order).astype(F32)
        square_total = square_total + lax.ppermute(square_tile, "tp", order)
    factor = lax.rsqrt(square_total[:, :1] / width + RMS_EPS)
    projected = total.transpose(2, 1, 0, 3).reshape(roles, seqs, chips_tp * wide) * factor[None]

    heads = part // HEAD

    def per_head(flat):
        return flat.reshape(seqs, heads, HEAD)

    receptance, key_vec, value_vec = (per_head(projected[i]) for i in range(3))
    decay_pre = per_head(projected[3] + decay_base)
    in_rate = jax.nn.sigmoid(per_head(projected[4] + rate_base))
    decay_rate = jnp.exp(-jnp.exp(-jax.nn.softplus(-decay_pre) - 0.5))
    unit_key = key_vec * lax.rsqrt(jnp.sum(key_vec * key_vec, axis=-1, keepdims=True) + KEY_EPS)
    carried = state.reshape(seqs, heads, HEAD, HEAD).astype(F32)
    removed = jnp.sum(carried * unit_key[:, :, None, :], axis=-1)
    kept = jnp.sum(carried * (decay_rate * receptance)[:, :, None, :], axis=-1)
    down_by = jnp.sum(unit_key * in_rate * receptance, axis=-1, keepdims=True)
    up_by = jnp.sum(key_vec * in_rate * receptance, axis=-1, keepdims=True)
    readout = kept - removed * down_by + value_vec * up_by
    centre = jnp.mean(readout, axis=-1, keepdims=True)
    spread = jnp.mean(jnp.square(readout - centre), axis=-1, keepdims=True)
    mixed = (readout - centre) * lax.rsqrt(spread + GN_EPS)
    mixed = (mixed.reshape(seqs, part) * head_gain).astype(BF16)

    mixed_rows = spread_rows(mixed).reshape(chips * seqs, part)
    own_o = jnp.dot(mixed_rows, w_out, preferred_element_type=F32)
    other_o = jnp.dot(mixed_rows, other_out, preferred_element_type=F32)
    first, second = both(own_o, other_o)
    partial = jnp.concatenate((first, second), axis=1)
    mine = lax.dynamic_slice_in_dim(rows, (chip % chips_tp) * wide, wide, 1).astype(F32)
    partial = partial + jnp.where(chip // chips_tp == shard, mine, 0.0)
    partial = partial.astype(BF16).reshape(chips, 1, seqs, wide)
    partial = jnp.broadcast_to(partial, (chips, tp, seqs, wide)).reshape(chips * tp, seqs, wide)
    back = lax.all_to_all(partial, ("chip", "tp"), 0, 0, tiled=True)
    resid = jnp.sum(back.reshape(chips, tp, seqs, wide).astype(F32), axis=1)
    resid = resid.transpose(1, 0, 2).reshape(seqs, width).astype(BF16)

    resid32 = resid.astype(F32)
    moe_factor = lax.rsqrt(jnp.mean(resid32 * resid32, axis=1, keepdims=True) + RMS_EPS)
    normed_two = (resid32 * moe_factor * moe_gain).astype(BF16)
    share = route_weight / jnp.sum(route_weight, axis=1, keepdims=True) * ROUTED_SCALE
    hit = routes[:, :, None] == jnp.arange(experts, dtype=jnp.int32)[None, None, :]
    table = jnp.sum(jnp.where(hit, share[:, :, None], 0.0), axis=1)
    table_high = table.astype(BF16)
    table_low = (table - table_high.astype(F32)).astype(BF16)
    tail = -(-2 * experts // 128) * 128
    pad = jnp.zeros((seqs, tail - 2 * experts), BF16)
    packed = jnp.concatenate((normed_two, table_high, table_low, pad), axis=1)
    arrived = spread_rows(packed).reshape(chips * seqs, width + tail)
    expert_in = arrived[:, :width]
    tables = arrived[:, width : width + 2 * experts].astype(F32)
    tables = tables[:, :experts] + tables[:, experts:]
    picks = jnp.arange(experts, dtype=jnp.int32)[None, :]

    def hidden_of(gate, up, expert):
        scale = jnp.sum(jnp.where(picks == expert, tables, 0.0), axis=1, keepdims=True)
        gate_val = jnp.dot(expert_in, gate, preferred_element_type=F32)
        up_val = jnp.dot(expert_in, up, preferred_element_type=F32)
        return (jax.nn.silu(gate_val) * up_val * scale).astype(BF16)

    me = chip * 2 + core
    own_h = hidden_of(expert_gate[0], expert_up[0], me)
    other_h = hidden_of(other_gate, other_up, chip * 2 + 1 - core)
    routed = jnp.dot(own_h, expert_down[0], preferred_element_type=F32)
    routed = routed + jnp.dot(other_h, other_down, preferred_element_type=F32)
    shared_hidden = (
        jax.nn.silu(jnp.dot(normed_two, shared_gate, preferred_element_type=F32))
        * jnp.dot(normed_two, shared_up, preferred_element_type=F32)
    ).astype(BF16)
    shared_part = jnp.dot(shared_hidden, shared_down, preferred_element_type=F32)
    at_home = jnp.arange(chips)[:, None, None] == chip
    routed = routed.reshape(chips, seqs, width) + jnp.where(at_home, shared_part[None], 0.0)
    routed = routed.astype(BF16).reshape(chips, seqs, tp, part).transpose(0, 2, 1, 3)
    routed = routed.reshape(chips * tp, seqs, part)
    returned = lax.all_to_all(routed, ("chip", "tp"), 0, 0, tiled=True)
    added = jnp.sum(returned.astype(F32), axis=0)
    own_resid = lax.dynamic_slice_in_dim(resid, shard * part, part, 1).astype(F32)
    return (own_resid + added).astype(BF16)


def solution(mesh):
    ep, tp = mesh.shape["ep"], mesh.shape["tp"]
    grid = Mesh(mesh.devices.reshape(ep // 2, 2, tp), ("chip", "core", "tp"))
    ep = ("chip", "core")
    placed = (
        P(ep, "tp"),
        P(ep, "tp", None),
        P("tp"),
        P("tp", ep),
        P("tp", ep),
        P("tp", ep),
        P("tp", ep),
        P("tp", ep),
        P("tp"),
        P("tp"),
        P("tp"),
        P("tp", ep),
        P(),
        P(ep, None),
        P(ep, None),
        P(ep, None, "tp"),
        P(ep, None, "tp"),
        P(ep, "tp", None),
        P(None, "tp"),
        P(None, "tp"),
        P("tp", None),
    )
    return jax.shard_map(body, mesh=grid, in_specs=placed, out_specs=P(ep, "tp"), check_vma=False)
```

time: 222 us -> 134 us (0.60)
  blocking collectives: 105 us -> 0 us
  starting transfers between devices: 9.27 us -> 31 us
  between operations: 13.6 us -> 0.53 us
  other arithmetic: 4.52 us -> 14.5 us
  waiting for transfers between devices: 46.1 us -> 53 us
  matrix products: 20.8 us -> 15.1 us
  local copies, waits for them, and re-layouts: 22.1 us -> 18.3 us
    all_gather x3 -> x0, blocking collectives: 51.2 us -> none  [the longest x2 46.6 us: project_split(): block_rows = lax.all_gather(part_rows, 'ep', axis=0, tiled=True)]
    all_to_all x2 -> x0, blocking collectives: 48 us -> none  [the longest x1 30.1 us: body(): lax.all_to_all(outgoing, 'ep', split_axis=0, concat_axis=0, tiled=True)]
    all_to_all x2 -> x6, waiting for transfers between devices: 16.4 us -> 49.9 us  [the longest x3 25.6 us: spread_rows(): return lax.all_to_all(copies, 'chip', 0, 0, tiled=True)]
    reduce_scatter x4 -> x0, waiting for transfers between devices: 29.7 us -> none  [quarter_sums(): lax.psum_scatter(for_sending(partial_value), 'tp', scatter_dimension=2, t...]
    all_to_all x2 -> x6, starting transfers between devices: 9.11 us -> 26.5 us  [the longest x3 14.1 us: spread_rows(): return lax.all_to_all(copies, 'chip', 0, 0, tiled=True)]
    reduce_sum x8 -> x9, other arithmetic: 1.24 us -> 7.75 us  [the longest x1 6.67 us: body(): removed = jnp.sum(carried * unit_key[:, :, None, :], axis=-1)]
    psum x1 -> x0, blocking collectives: 5.89 us -> none  [body(): square_sum = lax.psum(jnp.sum(tokens32 * tokens32, axis=1), 'tp')]
    reshape x8 -> x3, local copies, waits for them, and re-layouts: 7.72 us -> 1.95 us  [the longest x1 0.89 us: body(): first = first.reshape(chips, seqs, roles, cols)]
  transfers between devices with their start and end apart: 6 -> 13, of which waited for: 5 -> 7; matrix products, arithmetic and copies ran while one was open for 5% -> 15% of each run, Pallas kernels for 0% -> 0%
where the time goes in v1:
time: 134 us; the launch traced here: 133 us
  waiting for transfers between devices  53 us (40%)
  starting transfers between devices  31 us (23%)
  local copies, waits for them, and re-layouts  18.3 us (14%)
  matrix products  15.1 us (11%)
  other arithmetic  14.5 us (11%)
    all_to_all x3, waiting for transfers between devices, spread_rows(): return lax.all_to_all(copies, 'chip', 0, 0, tiled=True)  25.6 us
    all_to_all x3, starting transfers between devices, spread_rows(): return lax.all_to_all(copies, 'chip', 0, 0, tiled=True)  14.1 us
    all_to_all x1, waiting for transfers between devices, body(): returned = lax.all_to_all(routed, ('chip', 'tp'), 0, 0, tiled=True)  13.9 us
    all_to_all x1, waiting for transfers between devices, body(): back = lax.all_to_all(partial, ('chip', 'tp'), 0, 0, tiled=True)  7.68 us
    reduce_sum x1, other arithmetic, body(): removed = jnp.sum(carried * unit_key[:, :, None, :], axis=-1)  6.67 us
    convert_element_type x1, local copies, waits for them, and re-layouts, body(): carried = state.reshape(seqs, heads, HEAD, HEAD).astype(F32)  5.51 us
    unnamed x33, local copies, waits for them, and re-layouts  4.38 us
    all_to_all x1, starting transfers between devices, body(): returned = lax.all_to_all(routed, ('chip', 'tp'), 0, 0, tiled=True)  4.3 us
  transfers between devices with their start and end apart: 13, of which 7 were waited for; matrix products, arithmetic and copies ran while one was open for 15% of the time, Pallas kernels for 0%

profile of v1, /device:TPU:0, one launch (start us, length us, event | category | flops | bytes accessed | tf_op | source)
XLA Modules:
  0.0 132.5 jit_solution(2479745696522533278)
XLA Ops:
  4.7 6.8 %all-to-all-start = ((bf16[8,16,1024]{2,1,0:T(8,128)(2,1)}), bf16[8,16,1024]{2,1,0:T(8,128)(2,1)S(1)}, u32[]{:S(2)}, u32[]{:S(2)}) async-start(bf16[8,16,1024]{2,1,0:T(8,128)(2,1)} %broadcast_in_dim.63), calls=%async_computation | async-start | bytes 524288 | tf_op jit(solution)/shard_map/all_to_all | solution.py:25
  11.5 9.6 %all-to-all-done = bf16[8,16,1024]{2,1,0:T(8,128)(2,1)S(1)} async-done(((bf16[8,16,1024]{2,1,0:T(8,128)(2,1)}), bf16[8,16,1024]{2,1,0:T(8,128)(2,1)S(1)}, u32[]{:S(2)}, u32[]{:S(2)}) %all-to-all-start) | async-done | bytes 262176 | tf_op jit(solution)/shard_map/all_to_all | solution.py:25
  21.4 1.7 %broadcast_select_fusion.1 = (bf16[128,640]{1,0:T(8,128)(2,1)S(1)}, bf16[128,640]{1,0:T(8,128)(2,1)S(1)}) fusion(bf16[128,640]{1,0:T(8,128)(2,1)S(1)} %convolution_convert_fusion.1, pred[]{:T(512)S(6)} %eq.58, bf16[1024,640]{1,0:T(8,128)(2,1)} %collective-permute-done, bf16[128,1024]{1,0:T(8,128)(2,1)S(1)} %bitcast.59, f32[1024]{0:T(1024)S(1)} %copy-done.7), kind=kOutput, calls=%fused_computation.34 | convolution fusion | flops 168411136 | bytes 2068481 | tf_op jit(solution)/shard_map/dot_general | solution.py:83
  27.1 4.1 %all-to-all-start.1 = ((bf16[8,16,5,256]{3,1,2,0:T(8,128)(2,1)}), bf16[8,16,5,256]{3,1,2,0:T(8,128)(2,1)}, u32[]{:S(2)}, u32[]{:S(2)}) async-start(bf16[8,16,5,256]{3,1,2,0:T(8,128)(2,1)} %copy.45), calls=%async_computation.1 | async-start | bytes 655360 | tf_op jit(solution)/shard_map/all_to_all | solution.py:88
  31.3 1.6 %collective-permute-start.2 = (f32[16,128]{0,1:T(8,128)S(1)}, f32[16,128]{0,1:T(8,128)}, u32[]{:S(2)}, u32[]{:S(2)}) collective-permute-start(f32[16,128]{0,1:T(8,128)S(1)} %broadcast_in_dim.64), channel_id=1, source_target_pairs={{0,1},{1,0},{2,3},{3,2},{4,5},{5,4},{6,7},{7,6},{8,9},{9,8},{10,11... | collective-permute-start | bytes 24584 | tf_op jit(solution)/shard_map/ppermute | solution.py:99
  33.0 5.5 %reshape.251 = f32[16,16,64,64]{3,2,1,0:T(8,128)} reshape(bf16[16,16,4096]{2,1,0:T(8,128)(2,1)S(1)} %copy-done.1) | data formatting | bytes 6291456 | tf_op jit(solution)/shard_map/convert_element_type | solution.py:113
  38.5 2.8 %all-to-all-done.1 = bf16[8,16,5,256]{3,1,2,0:T(8,128)(2,1)} async-done(((bf16[8,16,5,256]{3,1,2,0:T(8,128)(2,1)}), bf16[8,16,5,256]{3,1,2,0:T(8,128)(2,1)}, u32[]{:S(2)}, u32[]{:S(2)}) %all-to-all-start.1) | async-done | bytes 327712 | tf_op jit(solution)/shard_map/all_to_all | solution.py:88
  42.4 1.6 %collective-permute-start.1 = (bf16[4,16,5,256]{3,0,1,2:T(4,128)(2,1)S(1)}, bf16[4,16,5,256]{3,0,1,2:T(4,128)(2,1)S(1)}, u32[]{:S(2)}, u32[]{:S(2)}) collective-permute-start(bf16[4,16,5,256]{3,0,1,2:T(4,128)(2,1)S(1)} %bitcast.69), channel_id=1, source_target_pairs={{0,1},{1,0},{2,3},{3,2},{4,5},{5,4},{6,7},{7,6},{8,9},{9,8},{10,11... | collective-permute-start | bytes 491528 | tf_op jit(solution)/shard_map/ppermute | solution.py:98
  44.7 3.1 %collective-permute-done.1 = bf16[4,16,5,256]{3,0,1,2:T(4,128)(2,1)S(1)} collective-permute-done((bf16[4,16,5,256]{3,0,1,2:T(4,128)(2,1)S(1)}, bf16[4,16,5,256]{3,0,1,2:T(4,128)(2,1)S(1)}, u32[]{:S(2)}, u32[]{:S(2)}) %collective-permute-start.1) | collective-permute-done | bytes 163872 | tf_op jit(solution)/shard_map/ppermute | solution.py:98
  49.0 6.7 %multiply_reduce_fusion = (f32[16,16,64]{2,1,0:T(8,128)S(1)}, f32[16,16,64]{2,1,0:T(8,128)S(1)}) fusion(f32[16,16,64,64]{3,2,1,0:T(8,128)} %reshape.251, f32[16,16,64]{2,1,0:T(8,128)S(1)} %get-tuple-element.14, f32[16,16,64]{2,1,0:T(8,128)S(1)} %get-tuple-element.28), kind=kLoop, calls=%fused_computation.1 | loop fusion | flops 4161536 | bytes 4456448 | tf_op jit(solution)/shard_map/reduce_sum | solution.py:114
  55.7 2.6 %fusion.37 = (f32[16,16]{1,0:T(8,128)S(1)}, f32[16,16,64]{2,1,0:T(8,128)S(1)}) fusion(f32[16,16,64]{2,1,0:T(8,128)S(1)} %reshape_squeeze.11, f32[16,16]{1,0:T(8,128)S(1)} %get-tuple-element.7, f32[16,16,64]{2,1,0:T(8,128)S(1)} %get-tuple-element.6, f32[16,16,64]{2,1,0:T(8,128)S(1)} %get-tuple-element.5, f32[16,16,64]{2,1,0:T(8,128)S(1)} %get-tuple-element.13), kind=kOutput, calls=%fused_computation.71 | output fusion | flops 81983 | bytes 329728 | tf_op jit(solution)/shard_map/mul | solution.py:118
  60.1 3.8 %all-to-all-start.2 = ((bf16[8,16,1024]{2,1,0:T(8,128)(2,1)}), bf16[8,16,1024]{2,1,0:T(8,128)(2,1)S(1)}, u32[]{:S(2)}, u32[]{:S(2)}) async-start(bf16[8,16,1024]{2,1,0:T(8,128)(2,1)} %broadcast_in_dim.66), calls=%async_computation.2 | async-start | bytes 524288 | tf_op jit(solution)/shard_map/all_to_all | solution.py:25
  64.2 7.9 %all-to-all-done.2 = bf16[8,16,1024]{2,1,0:T(8,128)(2,1)S(1)} async-done(((bf16[8,16,1024]{2,1,0:T(8,128)(2,1)}), bf16[8,16,1024]{2,1,0:T(8,128)(2,1)S(1)}, u32[]{:S(2)}, u32[]{:S(2)}) %all-to-all-start.2) | async-done | bytes 262176 | tf_op jit(solution)/shard_map/all_to_all | solution.py:25
  73.4 4.0 %all-to-all-start.3 = ((bf16[16,16,256]{2,1,0:T(8,128)(2,1)}), bf16[16,16,256]{2,1,0:T(8,128)(2,1)S(1)}, u32[]{:S(2)}, u32[]{:S(2)}) async-start(bf16[16,16,256]{2,1,0:T(8,128)(2,1)} %bitcast.9), calls=%async_computation.3 | async-start | bytes 262144 | tf_op jit(solution)/shard_map/all_to_all | solution.py:133
  77.6 7.7 %all-to-all-done.3 = bf16[16,16,256]{2,1,0:T(8,128)(2,1)S(1)} async-done(((bf16[16,16,256]{2,1,0:T(8,128)(2,1)}), bf16[16,16,256]{2,1,0:T(8,128)(2,1)S(1)}, u32[]{:S(2)}, u32[]{:S(2)}) %all-to-all-start.3) | async-done | bytes 131104 | tf_op jit(solution)/shard_map/all_to_all | solution.py:133
  86.5 3.5 %all-to-all-start.4 = ((bf16[8,16,2176]{2,1,0:T(8,128)(2,1)}), bf16[8,16,2176]{2,1,0:T(8,128)(2,1)S(1)}, u32[]{:S(2)}, u32[]{:S(2)}) async-start(bf16[8,16,2176]{2,1,0:T(8,128)(2,1)} %broadcast_in_dim.123), calls=%async_computation.4 | async-start | bytes 1114112 | tf_op jit(solution)/shard_map/all_to_all | solution.py:25
  92.2 2.0 %fusion.7 = f32[16,2048]{1,0:T(8,128)S(1)} fusion(bf16[256,2048]{1,0:T(8,128)(2,1)S(1)} %copy-done, bf16[16,2048]{1,0:T(8,128)(2,1)S(1)} %multiply_convert_fusion.4, bf16[2048,256]{1,0:T(8,128)(2,1)} %param.40, f32[16,256]{1,0:T(8,128)S(1)} %fusion.59), kind=kOutput, calls=%fused_computation.14 | convolution fusion | flops 33579008 | bytes 2310144 | tf_op jit(solution)/shard_map/dot_general | solution.py:169
  94.2 8.1 %all-to-all-done.4 = bf16[8,16,2176]{2,1,0:T(8,128)(2,1)S(1)} async-done(((bf16[8,16,2176]{2,1,0:T(8,128)(2,1)}), bf16[8,16,2176]{2,1,0:T(8,128)(2,1)S(1)}, u32[]{:S(2)}, u32[]{:S(2)}) %all-to-all-start.4) | async-done | bytes 557088 | tf_op jit(solution)/shard_map/all_to_all | solution.py:25
  102.4 1.5 %fusion.14 = f32[128,256]{1,0:T(8,128)S(1)} fusion(bf16[128,2176]{1,0:T(8,128)(2,1)S(1)} %bitcast.53, bf16[1,2048,256]{2,1,0:T(8,128)(2,1)} %param.36), kind=kOutput, calls=%fused_computation.26 | convolution fusion | flops 134217728 | bytes 1703936 | tf_op jit(solution)/shard_map/dot_general | solution.py:156
  104.0 1.5 %fusion.8 = f32[128,256]{1,0:T(8,128)S(1)} fusion(bf16[2048,256]{1,0:T(8,128)(2,1)} %collective-permute-done.5, bf16[128,2176]{1,0:T(8,128)(2,1)S(1)} %bitcast.54), kind=kOutput, calls=%fused_computation.21 | convolution fusion | flops 134217728 | bytes 1703936 | tf_op jit(solution)/shard_map/dot_general | solution.py:157
  105.5 3.4 %fusion.5 = f32[128,2048]{1,0:T(8,128)} fusion(bf16[128,2176]{1,0:T(8,128)(2,1)S(1)} %bitcast.55, f32[128,256]{1,0:T(8,128)S(1)} %fusion.14, f32[128]{0:T(128)S(1)} %get-tuple-element.10, bf16[1,256,2048]{2,1,0:T(8,128)(2,1)} %param.38, bf16[1,2048,256]{2,1,0:T(8,128)(2,1)} %param.37), kind=kOutput, calls=%fused_computation.11 | convolution fusion | flops 268664832 | bytes 3801600 | tf_op jit(solution)/shard_map/dot_general | solution.py:163
  109.9 2.6 %convolution_add_fusion = f32[128,2048]{1,0:T(8,128)S(1)} fusion(f32[128,2048]{1,0:T(8,128)} %fusion.5, bf16[256,2048]{1,0:T(8,128)(2,1)} %collective-permute-done.6, f32[128,256]{1,0:T(8,128)S(1)} %fusion.8, bf16[2048,256]{1,0:T(8,128)(2,1)} %copy-done.2, bf16[128,2176]{1,0:T(8,128)(2,1)S(1)} %bitcast.56, f32[128]{0:T(128)S(1)} %get-tuple-element.9), kind=kOutput, calls=%fused_computation.3 | convolution fusion | flops 268926976 | bytes 4850176 | tf_op jit(solution)/shard_map/dot_general | solution.py:164
  113.6 4.3 %all-to-all-start.5 = ((bf16[16,16,1024]{2,1,0:T(8,128)(2,1)}), bf16[16,16,1024]{2,1,0:T(8,128)(2,1)S(1)}, u32[]{:S(2)}, u32[]{:S(2)}) async-start(bf16[16,16,1024]{2,1,0:T(8,128)(2,1)} %bitcast.17), calls=%async_computation.5 | async-start | bytes 1048576 | tf_op jit(solution)/shard_map/all_to_all | solution.py:174
  117.9 13.9 %all-to-all-done.5 = bf16[16,16,1024]{2,1,0:T(8,128)(2,1)S(1)} async-done(((bf16[16,16,1024]{2,1,0:T(8,128)(2,1)}), bf16[16,16,1024]{2,1,0:T(8,128)(2,1)S(1)}, u32[]{:S(2)}, u32[]{:S(2)}) %all-to-all-start.5) | async-done | bytes 524320 | tf_op jit(solution)/shard_map/all_to_all | solution.py:174
  (110 shorter events, 21.7 us)
Async XLA Ops:
  0.0 92.2 %copy-start = (bf16[256,2048]{1,0:T(8,128)(2,1)S(1)}, bf16[256,2048]{1,0:T(8,128)(2,1)}, u32[]{:S(2)}) copy-start(bf16[256,2048]{1,0:T(8,128)(2,1)} %param.41) | copy-start | bytes 3145732
  0.0 3.9 %copy-start.6 = (bf16[16,1024]{1,0:T(8,128)(2,1)S(1)}, bf16[16,1024]{1,0:T(8,128)(2,1)}, u32[]{:S(2)}) copy-start(bf16[16,1024]{1,0:T(8,128)(2,1)} %param.21) | copy-start | bytes 98308
  2.1 18.9 %copy-start.7 = (f32[1024]{0:T(1024)S(1)}, f32[1024]{0:T(1024)}, u32[]{:S(2)}) copy-start(f32[1024]{0:T(1024)} %param.23) | copy-start | bytes 12292
  3.3 18.1 %collective-permute-start = (bf16[1024,640]{1,0:T(8,128)(2,1)S(1)}, bf16[1024,640]{1,0:T(8,128)(2,1)}, u32[]{:S(2)}, u32[]{:S(2)}) collective-permute-start(bf16[1024,640]{1,0:T(8,128)(2,1)S(1)} %constant_dynamic-update-slice_fusion), channel_id=1, source_target_pairs={{0,2},{2,0},{1,3},{3,1},{4,6},{6,4},{5,7},{7,5},{8,10},{10,8},{9,1... | collective-permute-start | bytes 3932168 | tf_op jit(solution)/shard_map/ppermute | solution.py:19
  4.7 16.4 %all-to-all-start = ((bf16[8,16,1024]{2,1,0:T(8,128)(2,1)}), bf16[8,16,1024]{2,1,0:T(8,128)(2,1)S(1)}, u32[]{:S(2)}, u32[]{:S(2)}) async-start(bf16[8,16,1024]{2,1,0:T(8,128)(2,1)} %broadcast_in_dim.63), calls=%async_computation | async-start | bytes 524288 | tf_op jit(solution)/shard_map/all_to_all | solution.py:25
  24.9 7.9 %copy-start.11 = (f32[1024]{0:T(1024)S(1)}, f32[1024]{0:T(1024)}, u32[]{:S(2)}) copy-start(f32[1024]{0:T(1024)} %param.30) | copy-start | bytes 12292
  24.9 8.0 %copy-start.12 = (f32[1024]{0:T(1024)S(1)}, f32[1024]{0:T(1024)}, u32[]{:S(2)}) copy-start(f32[1024]{0:T(1024)} %param.29) | copy-start | bytes 12292
  24.9 8.1 %copy-start.1 = (bf16[16,16,4096]{2,1,0:T(8,128)(2,1)S(1)}, bf16[16,16,4096]{2,1,0:T(8,128)(2,1)}, u32[]{:S(2)}) copy-start(bf16[16,16,4096]{2,1,0:T(8,128)(2,1)} %param.22) | copy-start | bytes 6291460
  27.1 14.2 %all-to-all-start.1 = ((bf16[8,16,5,256]{3,1,2,0:T(8,128)(2,1)}), bf16[8,16,5,256]{3,1,2,0:T(8,128)(2,1)}, u32[]{:S(2)}, u32[]{:S(2)}) async-start(bf16[8,16,5,256]{3,1,2,0:T(8,128)(2,1)} %copy.45), calls=%async_computation.1 | async-start | bytes 655360 | tf_op jit(solution)/shard_map/all_to_all | solution.py:88
  31.3 12.7 %collective-permute-start.2 = (f32[16,128]{0,1:T(8,128)S(1)}, f32[16,128]{0,1:T(8,128)}, u32[]{:S(2)}, u32[]{:S(2)}) collective-permute-start(f32[16,128]{0,1:T(8,128)S(1)} %broadcast_in_dim.64), channel_id=1, source_target_pairs={{0,1},{1,0},{2,3},{3,2},{4,5},{5,4},{6,7},{7,6},{8,9},{9,8},{10,11... | collective-permute-start | bytes 24584 | tf_op jit(solution)/shard_map/ppermute | solution.py:99
  42.4 5.4 %collective-permute-start.1 = (bf16[4,16,5,256]{3,0,1,2:T(4,128)(2,1)S(1)}, bf16[4,16,5,256]{3,0,1,2:T(4,128)(2,1)S(1)}, u32[]{:S(2)}, u32[]{:S(2)}) collective-permute-start(bf16[4,16,5,256]{3,0,1,2:T(4,128)(2,1)S(1)} %bitcast.69), channel_id=1, source_target_pairs={{0,1},{1,0},{2,3},{3,2},{4,5},{5,4},{6,7},{7,6},{8,9},{9,8},{10,11... | collective-permute-start | bytes 491528 | tf_op jit(solution)/shard_map/ppermute | solution.py:98
  55.7 3.6 %copy-start.10 = (f32[1024]{0:T(1024)S(1)}, f32[1024]{0:T(1024)}, u32[]{:S(2)}) copy-start(f32[1024]{0:T(1024)} %param.31) | copy-start | bytes 12292
  58.3 5.5 %copy-start.5 = (bf16[1024,128]{1,0:T(8,128)(2,1)S(1)}, bf16[1024,128]{1,0:T(8,128)(2,1)}, u32[]{:S(2)}) copy-start(bf16[1024,128]{1,0:T(8,128)(2,1)} %param.32) | copy-start | bytes 786436
  58.5 5.5 %copy-start.8 = (f32[16,6]{0,1:T(8,128)S(1)}, f32[16,6]{0,1:T(8,128)}, u32[]{:S(2)}) copy-start(f32[16,6]{0,1:T(8,128)} %param.35) | copy-start | bytes 1156
  60.1 12.0 %all-to-all-start.2 = ((bf16[8,16,1024]{2,1,0:T(8,128)(2,1)}), bf16[8,16,1024]{2,1,0:T(8,128)(2,1)S(1)}, u32[]{:S(2)}, u32[]{:S(2)}) async-start(bf16[8,16,1024]{2,1,0:T(8,128)(2,1)} %broadcast_in_dim.66), calls=%async_computation.2 | async-start | bytes 524288 | tf_op jit(solution)/shard_map/all_to_all | solution.py:25
  63.9 13.6 %copy-start.13 = (s32[16,6]{0,1:T(8,128)S(1)}, s32[16,6]{0,1:T(8,128)}, u32[]{:S(2)}) copy-start(s32[16,6]{0,1:T(8,128)} %param.34) | copy-start | bytes 1156
  63.9 8.5 %collective-permute-start.3 = (bf16[1024,128]{1,0:T(8,128)(2,1)S(1)}, bf16[1024,128]{1,0:T(8,128)(2,1)S(1)}, u32[]{:S(2)}, u32[]{:S(2)}) collective-permute-start(bf16[1024,128]{1,0:T(8,128)(2,1)S(1)} %copy-done.5), channel_id=1, source_target_pairs={{0,2},{2,0},{1,3},{3,1},{4,6},{6,4},{5,7},{7,5},{8,10},{10,8},{9,1... | collective-permute-start | bytes 786440 | tf_op jit(solution)/shard_map/ppermute | solution.py:19
  64.2 21.3 %copy-start.9 = (f32[2048]{0:T(1024)S(1)}, f32[2048]{0:T(1024)}, u32[]{:S(2)}) copy-start(f32[2048]{0:T(1024)} %param.33) | copy-start | bytes 24580
  73.4 11.9 %all-to-all-start.3 = ((bf16[16,16,256]{2,1,0:T(8,128)(2,1)}), bf16[16,16,256]{2,1,0:T(8,128)(2,1)S(1)}, u32[]{:S(2)}, u32[]{:S(2)}) async-start(bf16[16,16,256]{2,1,0:T(8,128)(2,1)} %bitcast.9), calls=%async_computation.3 | async-start | bytes 262144 | tf_op jit(solution)/shard_map/all_to_all | solution.py:133
  86.5 15.7 %all-to-all-start.4 = ((bf16[8,16,2176]{2,1,0:T(8,128)(2,1)}), bf16[8,16,2176]{2,1,0:T(8,128)(2,1)S(1)}, u32[]{:S(2)}, u32[]{:S(2)}) async-start(bf16[8,16,2176]{2,1,0:T(8,128)(2,1)} %broadcast_in_dim.123), calls=%async_computation.4 | async-start | bytes 1114112 | tf_op jit(solution)/shard_map/all_to_all | solution.py:25
  90.1 13.9 %collective-permute-start.5 = (bf16[2048,256]{1,0:T(8,128)(2,1)}, bf16[2048,256]{1,0:T(8,128)(2,1)}, u32[]{:S(2)}, u32[]{:S(2)}) collective-permute-start(bf16[2048,256]{1,0:T(8,128)(2,1)} %bitcast.14), channel_id=1, source_target_pairs={{0,2},{2,0},{1,3},{3,1},{4,6},{6,4},{5,7},{7,5},{8,10},{10,8},{9,1... | collective-permute-start | bytes 3145736 | tf_op jit(solution)/shard_map/ppermute | solution.py:19
  90.1 18.8 %collective-permute-start.4 = (bf16[2048,256]{1,0:T(8,128)(2,1)}, bf16[2048,256]{1,0:T(8,128)(2,1)S(1)}, u32[]{:S(2)}, u32[]{:S(2)}) collective-permute-start(bf16[2048,256]{1,0:T(8,128)(2,1)} %bitcast.63), channel_id=1, source_target_pairs={{0,2},{2,0},{1,3},{3,1},{4,6},{6,4},{5,7},{7,5},{8,10},{10,8},{9,1... | collective-permute-start | bytes 3145736 | tf_op jit(solution)/shard_map/ppermute | solution.py:19
  90.6 18.3 %collective-permute-start.6 = (bf16[256,2048]{1,0:T(8,128)(2,1)}, bf16[256,2048]{1,0:T(8,128)(2,1)}, u32[]{:S(2)}, u32[]{:S(2)}) collective-permute-start(bf16[256,2048]{1,0:T(8,128)(2,1)} %bitcast.64), channel_id=1, source_target_pairs={{0,2},{2,0},{1,3},{3,1},{4,6},{6,4},{5,7},{7,5},{8,10},{10,8},{9,1... | collective-permute-start | bytes 3145736 | tf_op jit(solution)/shard_map/ppermute | solution.py:19
  113.6 18.2 %all-to-all-start.5 = ((bf16[16,16,1024]{2,1,0:T(8,128)(2,1)}), bf16[16,16,1024]{2,1,0:T(8,128)(2,1)S(1)}, u32[]{:S(2)}, u32[]{:S(2)}) async-start(bf16[16,16,1024]{2,1,0:T(8,128)(2,1)} %bitcast.17), calls=%async_computation.5 | async-start | bytes 1048576 | tf_op jit(solution)/shard_map/all_to_all | solution.py:174
  (3 other events, 7.4 us)

commit v2 on v1

v2 whole, which is shorter than its diff:
```python
import functools

import jax
import jax.numpy as jnp
from jax import lax
from jax.experimental import pallas as pl
from jax.experimental.pallas import tpu as pltpu
from jax.sharding import Mesh, PartitionSpec as P

HEAD = 64
LANES = 128


RMS_EPS = 1e-06
GN_EPS = 0.00064
KEY_EPS = 1e-06
ROUTED_SCALE = 2.5

F32 = jnp.float32
BF16 = jnp.bfloat16


def dot(left, right):
    return jnp.dot(left, right, preferred_element_type=F32)


def paired(index, step, count):
    if count & (count - 1) == 0:
        return index ^ step
    return (step - index) % count


def swap_pairs(array, axis, step):
    count = lax.axis_size(axis)
    return lax.ppermute(array, axis, [(i, paired(i, step, count)) for i in range(count)])


def spread_rows(rows):
    copies = jnp.broadcast_to(rows[None], (lax.axis_size("z") * lax.axis_size("x"),) + rows.shape)
    return lax.all_to_all(copies, ("z", "x"), 0, 0, tiled=True)


class Late:
    def __init__(self, source, held, arrival):
        self.held, self.shape = held, held.shape
        self.copy = pltpu.make_async_copy(source, held, arrival)
        self.copy.start()
        self.waited = False

    def __getitem__(self, index):
        if not self.waited:
            self.copy.wait()
            self.waited = True
        return self.held[index]


def call(kernel, outs, place, *operands, scratch=(), late=()):
    hbm, vmem = (pl.BlockSpec(memory_space=space) for space in (pltpu.HBM, pltpu.VMEM))
    leaves, tree = jax.tree.flatten(outs)
    counts = len(operands), len(late), len(leaves), len(scratch)
    operands = [pltpu.with_memory_space_constraint(array, pltpu.VMEM) for array in operands]
    later = [pltpu.with_memory_space_constraint(array, pltpu.HBM) for array in late]
    buffers = [pltpu.VMEM(array.shape, array.dtype) for array in late]
    if late:
        buffers.append(pltpu.SemaphoreType.DMA((len(late),)))

    def with_copies(place, *refs):
        parts = []
        for count in counts:
            parts.append(refs[:count])
            refs = refs[count:]
        given, sources, results, own = parts
        waiting = [
            Late(source, held, refs[-1].at[index])
            for index, (source, held) in enumerate(zip(sources, refs))
        ]
        kernel(place, *given, *waiting, *results, *own)

    return pl.pallas_call(
        with_copies,
        out_shape=jax.tree.unflatten(
            tree, [pltpu.VMEM(leaf.shape, leaf.dtype) for leaf in leaves]
        ),
        in_specs=[pl.BlockSpec(memory_space=pltpu.SMEM)]
        + [vmem] * len(operands)
        + [hbm] * len(later),
        out_specs=jax.tree.map(lambda _: vmem, outs),
        scratch_shapes=list(scratch) + buffers,
        compiler_params=pltpu.CompilerParams(vmem_limit_bytes=24 * 1024 * 1024),
    )(place, *operands, *later)


def fetch_kernel(*refs):
    count = len(refs) // 2
    sources, held, arrivals = refs[:count], refs[count : 2 * count], refs[2 * count]
    copies = [
        pltpu.make_async_copy(source, target, arrivals.at[index])
        for index, (source, target) in enumerate(zip(sources, held))
    ]
    for copy in copies:
        copy.start()
    for copy in copies:
        copy.wait()


def fetch(*arrays):
    return pl.pallas_call(
        fetch_kernel,
        out_shape=[pltpu.VMEM(array.shape, array.dtype) for array in arrays],
        in_specs=[pl.BlockSpec(memory_space=pltpu.HBM)] * len(arrays),
        out_specs=[pl.BlockSpec(memory_space=pltpu.VMEM)] * len(arrays),
        scratch_shapes=[pltpu.SemaphoreType.DMA((len(arrays),))],
        compiler_params=pltpu.CompilerParams(vmem_limit_bytes=24 * 1024 * 1024),
    )(*(pltpu.with_memory_space_constraint(array, pltpu.HBM) for array in arrays))


def square_holder(target, tp, chips_tp):
    return (target + 1) % tp * chips_tp


def project_kernel(sizes, place, rows, gain, *refs):
    tp, chips_tp, roles = sizes
    other, own, out = refs[:roles], refs[roles : 2 * roles], refs[2 * roles]
    core = place[2]
    chips, seqs, part = rows.shape
    cols = own[0].shape[1]
    chip = place[0] * place[4] + place[1]
    group = chip // chips_tp
    count = chips * seqs
    left = rows[...].astype(F32).reshape(count, part)
    square = jnp.sum(left * left, axis=1, keepdims=True)
    high = square.astype(BF16)
    low = (square - high.astype(F32)).astype(BF16)
    scaled = (left * gain[...]).astype(BF16)
    for shift in range(1, tp):
        target = (group + shift) % tp
        for index, vals in enumerate((high, low)):
            vals = jnp.broadcast_to(vals.astype(F32), (count, cols)).astype(BF16)
            out[:, target, 0, index] = vals.reshape(chips, seqs, cols)
    for role in range(roles):
        weight = jnp.concatenate((own[role][...], other[role][...]), axis=1)
        product = dot(scaled, weight).astype(BF16).reshape(chips, seqs, 2 * cols)
        out[:, group, role, core] = product[:, :, :cols]
        out[:, group, role, 1 - core] = product[:, :, cols:]


def project(kernels, place, rows, gain, own, other, tp):
    chips, seqs, part = rows.shape
    cols = own[0].shape[1]
    roles = len(own)
    chips_tp = chips // tp
    shape = (chips, tp, roles, 2, seqs, cols)
    if kernels:
        kernel = functools.partial(project_kernel, (tp, chips_tp, roles))
        out = jax.ShapeDtypeStruct(shape, BF16)
        return call(kernel, out, place, rows, gain, *other, late=own)
    core = place[2]
    group = (place[0] * place[4] + place[1]) // chips_tp
    scaled = (rows.astype(F32) * gain[0]).astype(BF16).reshape(chips * seqs, part)
    pairs = []
    for mine, theirs in zip(own, other):
        sides = jnp.stack((dot(scaled, mine), dot(scaled, theirs))).astype(BF16)
        pairs.append(jnp.where(core == 0, sides, sides[::-1]))
    product = jnp.stack(pairs).reshape(roles, 2, chips, seqs, cols).transpose(2, 0, 1, 3, 4)
    square = jnp.sum(jnp.square(rows.astype(F32)), axis=2)
    high = square.astype(BF16)
    low = (square - high.astype(F32)).astype(BF16)
    marks = jnp.stack((high, low), axis=1)[:, None, :, :, None]
    marks = jnp.broadcast_to(marks, (chips, roles, 2, seqs, cols))
    here = (jnp.arange(tp) == group)[None, :, None, None, None, None]
    return jnp.where(here, product[:, None], marks[:, None])


def gates(decay_pre, rate_pre):
    decay_rate = jnp.exp(-jnp.exp(-jax.nn.softplus(-decay_pre) - 0.5))
    return decay_rate, jax.nn.sigmoid(rate_pre)


def mixer_kernel(place, got, state, decay_base, rate_base, head_gain, out, products, flat):
    chips, tp, _, _, seqs, cols = got.shape
    chips_tp = chips // tp
    heads = state.shape[1]
    count = seqs * heads
    half = count // 2
    shard = place[3]
    holder = square_holder(shard, tp, chips_tp)
    square = jnp.zeros((seqs, cols), F32)
    for source in range(tp):
        for index in range(2):
            square = square + got[holder, source, 0, index].astype(F32)
    factor = lax.rsqrt(square / (heads * HEAD * tp) + RMS_EPS)

    def role(index, base=None):
        vals = jnp.zeros((chips_tp, 2, seqs, cols), F32)
        for source in range(tp):
            vals = vals + got[pl.ds(shard * chips_tp, chips_tp), source, index].astype(F32)
        vals = vals * factor
        if base is not None:
            vals = vals + base[...]
        return vals.reshape(half, LANES)

    receptance, key_vec, value_vec = role(0), role(1), role(2)
    decay_rate, in_rate = gates(role(3, decay_base), role(4, rate_base))
    row = lax.broadcasted_iota(jnp.int32, (LANES, LANES), 0)
    lane = lax.broadcasted_iota(jnp.int32, (LANES, LANES), 1)
    same_head = (row // HEAD == lane // HEAD).astype(F32)

    def head_sum(vals):
        return jnp.dot(
            vals, same_head, precision=lax.Precision.HIGHEST, preferred_element_type=F32
        )

    unit_key = key_vec * lax.rsqrt(head_sum(key_vec * key_vec) + KEY_EPS)
    steer = in_rate * receptance
    down_by = head_sum(unit_key * steer)
    raised = value_vec * head_sum(key_vec * steer)
    side = lax.broadcasted_iota(jnp.int32, (half, LANES), 1) < HEAD
    evens, odds = [], []
    for vals in (decay_rate * receptance, unit_key, raised, down_by):
        turned = pltpu.roll(vals, HEAD, 1)
        evens.append(jnp.where(side, vals, turned))
        odds.append(jnp.where(side, turned, vals))
    stacked = jnp.concatenate(
        (jnp.concatenate(evens, axis=1), jnp.concatenate(odds, axis=1)), axis=0
    )
    high = stacked.astype(BF16)
    low = (stacked - high.astype(F32)).astype(BF16)
    row = lax.broadcasted_iota(jnp.int32, (count, count), 0)
    col = lax.broadcasted_iota(jnp.int32, (count, count), 1)
    block = (col % half) // seqs
    chosen = (row // heads == col % seqs) & (row % heads == 2 * block + col // half)
    chosen = chosen.astype(F32).astype(BF16)
    turned = dot(chosen, high) + dot(chosen, low)
    along, unit, raised, down_by = (
        turned[:, index * LANES : (index + 1) * LANES] for index in range(4)
    )
    along = jnp.concatenate((along, along), axis=1)
    unit = jnp.concatenate((unit, unit), axis=1)
    span = 2 * LANES
    for start in range(0, HEAD * HEAD, span):
        vals = state[:, :, start : start + span].reshape(count, span).astype(F32)
        products[:count, start : start + span] = (vals * along).astype(BF16)
        products[count:, start : start + span] = (vals * unit).astype(BF16)
    row = lax.broadcasted_iota(jnp.int32, (HEAD * HEAD, HEAD), 0)
    col = lax.broadcasted_iota(jnp.int32, (HEAD * HEAD, HEAD), 1)
    sums = dot(products[...], (row // HEAD == col).astype(F32).astype(BF16))
    readout = sums[:count] - sums[count:] * down_by[:, :HEAD] + raised[:, :HEAD]
    readout = readout - jnp.mean(readout, axis=-1, keepdims=True)
    spread = jnp.mean(readout * readout, axis=-1, keepdims=True)
    normed = readout * lax.rsqrt(spread + GN_EPS)
    gain = jnp.broadcast_to(head_gain[...][None], (seqs, heads, HEAD)).reshape(count, HEAD)
    flat[...] = normed * gain
    for index in range(0, heads, 2):
        first = flat[pl.ds(index, seqs, stride=heads), :]
        second = flat[pl.ds(index + 1, seqs, stride=heads), :]
        out[:, index * HEAD : (index + 2) * HEAD] = jnp.concatenate((first, second), axis=1).astype(
            BF16
        )


def mixer(kernels, place, got, state, decay_base, rate_base, head_gain):
    seqs, heads, _ = state.shape
    chips, tp, roles, _, _, cols = got.shape
    chips_tp = chips // tp
    part = heads * HEAD
    if kernels:
        return call(
            mixer_kernel,
            jax.ShapeDtypeStruct((seqs, part), BF16),
            place,
            got,
            state,
            decay_base,
            rate_base,
            head_gain,
            scratch=(
                pltpu.VMEM((2 * seqs * heads, HEAD * HEAD), BF16),
                pltpu.VMEM((seqs * heads, HEAD), F32),
            ),
        )
    shard = place[3]
    holder = square_holder(shard, tp, chips_tp)
    square = lax.dynamic_index_in_dim(got, holder, 0, keepdims=False)[:, 0].astype(F32)
    factor = lax.rsqrt(jnp.sum(square, axis=(0, 1))[:, :1] / (part * tp) + RMS_EPS)
    total = lax.dynamic_slice_in_dim(got, shard * chips_tp, chips_tp, 0)
    total = jnp.sum(total.astype(F32), axis=1) * factor
    total = total.transpose(1, 3, 0, 2, 4).reshape(roles, seqs, part)

    def per_head(vals):
        return vals.reshape(-1, heads, HEAD)

    receptance, key_vec, value_vec = (per_head(total[i]) for i in range(3))
    decay_rate, in_rate = gates(
        per_head(total[3]) + per_head(decay_base), per_head(total[4]) + per_head(rate_base)
    )
    unit_key = key_vec * lax.rsqrt(jnp.sum(key_vec * key_vec, axis=-1, keepdims=True) + KEY_EPS)
    carried = state.reshape(seqs, heads, HEAD, HEAD).astype(F32)
    removed = jnp.sum(carried * unit_key[:, :, None, :], axis=-1)
    kept = jnp.sum(carried * (decay_rate * receptance)[:, :, None, :], axis=-1)
    steer = in_rate * receptance
    down_by = jnp.sum(unit_key * steer, axis=-1, keepdims=True)
    up_by = jnp.sum(key_vec * steer, axis=-1, keepdims=True)
    readout = kept - removed * down_by + value_vec * up_by
    centre = jnp.mean(readout, axis=-1, keepdims=True)
    spread = jnp.mean(jnp.square(readout - centre), axis=-1, keepdims=True)
    mixed = (readout - centre) * lax.rsqrt(spread + GN_EPS)
    return (mixed * head_gain).reshape(seqs, part).astype(BF16)


def attend_kernel(sizes, place, rows, *refs):
    z_size, x_size, tp = sizes
    lines, weights, out = refs[:z_size], refs[-2:-1] + refs[z_size:-2], refs[-1]
    z, x, core, shard = (place[index] for index in range(4))
    seqs, cols = lines[0].shape[0], weights[0].shape[1]
    z_tp = z_size // tp
    left = jnp.concatenate([line[...] for line in lines], axis=0)
    holds = (z // z_tp == shard).astype(F32)
    for step in range(x_size):
        weight = jnp.concatenate([ref[...] for ref in weights[2 * step : 2 * step + 2]], axis=1)
        product = dot(left, weight)
        for side in range(2):
            slot = paired(x, step, x_size) * 2 + (core ^ side)
            offset = pl.multiple_of(((z % z_tp) * 2 * x_size + slot) * cols, cols)
            for line in range(z_size):
                z_to = paired(z, line, z_size)
                token = rows[z_to * x_size + x, :, pl.ds(offset, cols)].astype(F32)
                vals = product[line * seqs : (line + 1) * seqs, side * cols : (side + 1) * cols]
                out[z_to, slot] = (vals + token * holds).astype(BF16)


def attend(kernels, place, rows, lines, weights, tp, x_size):
    z_size = len(lines)
    seqs, part = lines[0].shape
    cols = weights[0].shape[1]
    shape = (z_size, 2 * x_size, seqs, cols)
    if kernels:
        kernel = functools.partial(attend_kernel, (z_size, x_size, tp))
        out = jax.ShapeDtypeStruct(shape, BF16)
        return call(kernel, out, place, rows, *lines, *weights[1:], late=weights[:1])
    z, x, core, shard = (place[index] for index in range(4))
    z_tp = z_size // tp
    z_order = jnp.stack([paired(z, i, z_size) for i in range(z_size)])
    x_order = jnp.stack([paired(x, i // 2, x_size) * 2 + (core ^ (i % 2)) for i in range(2 * x_size)])
    left = jnp.take(jnp.stack(lines), z_order, axis=0).reshape(z_size * seqs, part)
    weight = jnp.take(jnp.stack(weights), jnp.argsort(x_order), axis=0)
    product = jnp.einsum("rk,skc->rsc", left, weight, preferred_element_type=F32)
    token = lax.dynamic_index_in_dim(
        rows.reshape(z_size, x_size, seqs, z_tp, 2 * x_size, cols), x, 1, keepdims=False
    )
    token = lax.dynamic_index_in_dim(token, z % z_tp, 2, keepdims=False).astype(F32)
    product = product.reshape(z_size, seqs, 2 * x_size, cols)
    product = product + jnp.where(z // z_tp == shard, token, 0.0)
    return product.astype(BF16).reshape(z_size, 1, seqs, 2 * x_size * cols)


def residual_kernel(place, tables, *refs):
    *parts, out = refs
    lines, slots, seqs, cols = parts[0].shape
    for line in range(lines):
        for slot in range(slots):
            vals = sum(part[line, slot].astype(F32) for part in parts).astype(BF16)
            for chip in range(out.shape[0]):
                out[chip, line * slots + slot] = vals
    for index in range(tables.shape[0]):
        for chip in range(out.shape[0]):
            out[chip, lines * slots + index] = tables[index]


def residual(kernels, place, parts, tables, chips):
    lines, slots, seqs, cols = parts[0].shape
    tiles = lines * slots + tables.shape[0]
    if kernels:
        shape = jax.ShapeDtypeStruct((chips, tiles, seqs, cols), BF16)
        return call(residual_kernel, shape, place, tables, *parts)
    total = sum(part.astype(F32) for part in parts).astype(BF16)
    total = jnp.concatenate((total.reshape(lines * slots, seqs, cols), tables), axis=0)
    return jnp.broadcast_to(total[None], (chips,) + total.shape)


def expert_kernel(sizes, place, got, gain, *refs):
    x_size, experts = sizes
    own, other, shared = refs[:3], refs[3:6], refs[6:9]
    out, resid, left, home = refs[9:]
    chips, tp, seqs, part = out.shape
    z_size = chips // x_size
    cols = got.shape[3]
    slots = 2 * x_size
    width = part * tp
    count = chips * seqs
    z, x, core, shard = (place[index] for index in range(4))
    chip = z * x_size + x
    for index in range(chips):
        z_to, x_from = divmod(index, x_size)
        square = jnp.zeros((seqs, cols), F32)
        pieces = []
        for z_from in range(z_size):
            for slot in range(slots):
                piece = got[z_from * x_size + x_from, z_to * slots + slot].astype(F32)
                square = square + piece * piece
                pieces.append(piece)
        factor = lax.rsqrt(jnp.sum(square, axis=1, keepdims=True) / width + RMS_EPS)
        for block, piece in enumerate(pieces):
            lanes = slice(block * cols, (block + 1) * cols)
            left[index, :, lanes] = (piece * factor * gain[:, lanes]).astype(BF16)
    for z_part in range(z_size // tp):
        for slot in range(slots):
            block = z_part * slots + slot
            source = (shard * (z_size // tp) + z_part) * x_size + x
            resid[:, block * cols : (block + 1) * cols] = got[source, z * slots + slot]
    rows = left[...].reshape(count, width)
    tables = [
        got[:, z_size * slots + index].astype(F32).reshape(count, cols)
        for index in range(got.shape[1] - z_size * slots)
    ]
    tables = tables[0] if len(tables) == 1 else jnp.concatenate(tables, axis=1)
    lane = lax.broadcasted_iota(jnp.int32, tables.shape, 1)

    def hidden_of(vals, weights):
        gate, up, _ = weights
        return jax.nn.silu(dot(vals, gate[...])) * dot(vals, up[...])

    def scaled(weights, expert):
        hit = (lane == expert) | (lane == experts + expert)
        scale = jnp.sum(jnp.where(hit, tables, 0.0), axis=1, keepdims=True)
        return (hidden_of(rows, weights) * scale).astype(BF16)

    own_hidden = scaled(own, chip * 2 + core)
    other_hidden = scaled(other, chip * 2 + 1 - core)
    home_hidden = hidden_of(left[chip], shared).astype(BF16)
    for target in range(tp):
        for start in range(0, part, 512):
            lanes = slice(start, min(start + 512, part))
            span = slice(target * part + lanes.start, target * part + lanes.stop)
            vals = dot(own_hidden, own[2][:, span]) + dot(other_hidden, other[2][:, span])
            vals = vals.reshape(chips, seqs, lanes.stop - lanes.start)
            home[...] = dot(home_hidden, shared[2][:, span])
            for index in range(chips):
                extra = jnp.where(chip == index, home[...], 0.0)
                out[index, target, :, lanes] = (vals[index] + extra).astype(BF16)


def expert_rows(kernels, place, got, gain, own, other, shared, tp, x_size):
    chips, _, seqs, cols = got.shape
    z_size = chips // x_size
    width = gain.shape[1]
    slots = width // (z_size * cols)
    part = width // tp
    experts = 2 * chips
    if kernels:
        kernel = functools.partial(expert_kernel, (x_size, experts))
        shapes = [
            jax.ShapeDtypeStruct((chips, tp, seqs, part), BF16),
            jax.ShapeDtypeStruct((seqs, part), BF16),
        ]
        scratch = (pltpu.VMEM((chips, seqs, width), BF16), pltpu.VMEM((seqs, 512), F32))
        return call(
            kernel, shapes, place, got, gain, *own, *other, scratch=scratch, late=shared
        )
    chip = place[0] * place[4] + place[1]
    rows = got[:, : z_size * slots].reshape(z_size, x_size, z_size, slots, seqs, cols)
    rows = rows.transpose(2, 1, 4, 0, 3, 5).reshape(chips, seqs, width)
    resid = lax.dynamic_index_in_dim(rows, chip, 0, keepdims=False)
    resid = lax.dynamic_slice_in_dim(resid, place[3] * part, part, 1)
    rows = rows.astype(F32)
    factor = lax.rsqrt(jnp.mean(rows * rows, axis=2, keepdims=True) + RMS_EPS)
    rows = (rows * factor * gain).astype(BF16)
    left = rows.reshape(chips * seqs, width)
    tables = got[:, z_size * slots :].astype(F32).transpose(0, 2, 1, 3).reshape(chips * seqs, -1)
    tables = tables[:, :experts] + tables[:, experts : 2 * experts]
    names = jnp.arange(experts, dtype=jnp.int32)[None, :]

    def hidden_of(vals, weights):
        gate, up, _ = weights
        return jax.nn.silu(dot(vals, gate)) * dot(vals, up)

    def product(weights, expert):
        scale = jnp.sum(jnp.where(names == expert, tables, 0.0), axis=1, keepdims=True)
        return dot((hidden_of(left, weights) * scale).astype(BF16), weights[2])

    routed = product(own, chip * 2 + place[2]) + product(other, chip * 2 + 1 - place[2])
    home = lax.dynamic_index_in_dim(rows, chip, 0, keepdims=False)
    home = dot(hidden_of(home, shared).astype(BF16), shared[2])
    here = jnp.arange(chips)[:, None, None] == chip
    routed = routed.reshape(chips, seqs, width) + jnp.where(here, home[None], 0.0)
    routed = routed.astype(BF16).reshape(chips, seqs, tp, part).transpose(0, 2, 1, 3)
    return routed, resid


def body(
    tokens,
    state,
    mix_gain,
    w_recept,
    w_key,
    w_value,
    w_decay,
    w_rate,
    decay_base,
    rate_base,
    head_gain,
    w_out,
    moe_gain,
    routes,
    route_weight,
    expert_gate,
    expert_up,
    expert_down,
    shared_gate,
    shared_up,
    shared_down,
):
    z_size, x_size, tp = (lax.axis_size(name) for name in ("z", "x", "tp"))
    chips = z_size * x_size
    seqs, part = tokens.shape
    width = part * tp
    cols = w_out.shape[1]
    experts = 2 * chips
    kernels = cols == LANES and seqs == 16 and part % LANES == 0
    z, x, core, shard = (lax.axis_index(name) for name in ("z", "x", "core", "tp"))
    place = (z, x, core, shard, x_size)
    if kernels:
        place = jnp.stack([jnp.int32(index) for index in place])

    rows = spread_rows(tokens)
    own_w = (w_recept, w_key, w_value, w_decay, w_rate)
    other_w = tuple(swap_pairs(weight, "core", 1) for weight in own_w)
    mix_gain = mix_gain.reshape(1, part)
    moe_gain = moe_gain.reshape(1, width)
    blocks = (chips // tp, 2, 1, cols)
    decay_base, rate_base = decay_base.reshape(blocks), rate_base.reshape(blocks)
    head_gain = head_gain.reshape(part // HEAD, HEAD)
    if kernels:
        mix_gain, moe_gain, decay_base, rate_base, head_gain, state = fetch(
            mix_gain, moe_gain, decay_base, rate_base, head_gain, state
        )
    sent = project(kernels, place, rows, mix_gain, own_w, other_w, tp)
    sent = sent.reshape((chips * tp,) + sent.shape[2:])
    got = lax.all_to_all(sent, ("z", "x", "tp"), 0, 0, tiled=True)
    got = got.reshape((chips, tp) + got.shape[1:])
    mixed = mixer(kernels, place, got, state, decay_base, rate_base, head_gain)

    out_w = []
    for step in range(x_size):
        weight = w_out if step == 0 else swap_pairs(w_out, "x", step)
        out_w += [weight, swap_pairs(weight, "core", 1)]
    lines = [mixed] + [swap_pairs(mixed, "z", step) for step in range(1, z_size)]
    partial = attend(kernels, place, rows, lines, out_w, tp, x_size)
    partials = [partial] + [swap_pairs(partial, "tp", step) for step in range(1, tp)]

    share = route_weight / jnp.sum(route_weight, axis=1, keepdims=True) * ROUTED_SCALE
    hit = routes[:, :, None] == jnp.arange(experts, dtype=jnp.int32)[None, None, :]
    table = jnp.sum(jnp.where(hit, share[:, :, None], 0.0), axis=1)
    high = table.astype(BF16)
    low = (table - high.astype(F32)).astype(BF16)
    lanes = partial.shape[3]
    pad = jnp.zeros((seqs, -(2 * experts) % lanes), BF16)
    tables = jnp.concatenate((high, low, pad), axis=1)
    tables = tables.reshape(seqs, -1, lanes).transpose(1, 0, 2)
    packed = residual(kernels, place, partials, tables, chips)
    got = lax.all_to_all(packed, ("z", "x"), 0, 0, tiled=True)

    own = (expert_gate[0], expert_up[0], expert_down[0])
    other = tuple(swap_pairs(weight, "core", 1) for weight in own)
    shared = (shared_gate, shared_up, shared_down)
    routed, resid = expert_rows(
        kernels, place, got, moe_gain, own, other, shared, tp, x_size
    )
    routed = routed.reshape(chips * tp, seqs, part)
    returned = lax.all_to_all(routed, ("z", "x", "tp"), 0, 0, tiled=True)
    return (resid.astype(F32) + jnp.sum(returned.astype(F32), axis=0)).astype(BF16)


def solution(mesh):
    ep, tp = mesh.shape["ep"], mesh.shape["tp"]
    lines = mesh.devices.reshape(ep // 2, 2, tp)
    x_size = len({getattr(device, "coords", (0,))[0] for device in lines[:, 0, 0]})
    grid = Mesh(lines.reshape(-1, x_size, 2, tp), ("z", "x", "core", "tp"))
    ep = ("z", "x", "core")
    placed = (
        P(ep, "tp"),
        P(ep, "tp", None),
        P("tp"),
        P("tp", ep),
        P("tp", ep),
        P("tp", ep),
        P("tp", ep),
        P("tp", ep),
        P("tp"),
        P("tp"),
        P("tp"),
        P("tp", ep),
        P(),
        P(ep, None),
        P(ep, None),
        P(ep, None, "tp"),
        P(ep, None, "tp"),
        P(ep, "tp", None),
        P(None, "tp"),
        P(None, "tp"),
        P("tp", None),
    )
    return jax.shard_map(body, mesh=grid, in_specs=placed, out_specs=P(ep, "tp"), check_vma=False)
```

time: 134 us -> 106 us (0.79)
  blocking collectives: 0 us -> 18.8 us
  waiting for transfers between devices: 53 us -> 34.6 us
  Pallas kernels: 0 us -> 18.1 us
  matrix products: 15.1 us -> 0 us
  local copies, waits for them, and re-layouts: 18.3 us -> 4.28 us
  other arithmetic: 14.5 us -> 4.07 us
  starting transfers between devices: 31 us -> 25.5 us
    all_to_all x6 -> x3, waiting for transfers between devices: 49.9 us -> 18.8 us  [the longest x1 12.8 us: body(): got = lax.all_to_all(packed, ('z', 'x'), 0, 0, tiled=True)]
    all_to_all x0 -> x1, blocking collectives: none -> 18.8 us  [body(): returned = lax.all_to_all(routed, ('z', 'x', 'tp'), 0, 0, tiled=True)]
    pallas_call x0 -> x6, Pallas kernels: none -> 18.1 us  [the longest x5 16.4 us: call(): pl.pallas_call(with_copies, out_shape=jax.tree.unflatten(tree, [pltpu.VME...]
    dot_general x10 -> x0, matrix products: 15.1 us -> none  [the longest x1 3.35 us: body(): routed = jnp.dot(own_h, expert_down[0], preferred_element_type=F32)]
    ppermute x7 -> x15, waiting for transfers between devices: 3.12 us -> 15.8 us  [swap_pairs(): lax.ppermute(array, axis, [(i, paired(i, step, count)) for i in range(cou...]
    all_to_all x6 -> x3, starting transfers between devices: 26.5 us -> 15.9 us  [the longest x1 7.28 us: spread_rows(): return lax.all_to_all(copies, ('z', 'x'), 0, 0, tiled=True)]
    reduce_sum x8 -> x1, other arithmetic: 7.66 us -> 0.08 us  [body(): jnp.sum(returned.astype(F32), axis=0)]
    convert_element_type x3 -> x0, local copies, waits for them, and re-layouts: 5.63 us -> none  [the longest x1 5.51 us: body(): carried = state.reshape(seqs, heads, HEAD, HEAD).astype(F32)]
  transfers between devices with their start and end apart: 13 -> 18, of which waited for: 7 -> 7; matrix products, arithmetic and copies ran while one was open for 15% -> 5% of each run, Pallas kernels for 0% -> 8%
where the time goes in v2:
time: 106 us; the launch traced here: 105 us
  waiting for transfers between devices  34.6 us (33%)
  starting transfers between devices  25.5 us (24%)
  blocking collectives  18.8 us (18%)
  Pallas kernels  18.1 us (17%)
  local copies, waits for them, and re-layouts  4.28 us (4%)
  other arithmetic  4.07 us (4%)
    all_to_all x1, blocking collectives, body(): returned = lax.all_to_all(routed, ('z', 'x', 'tp'), 0, 0, tiled=True)  18.8 us
    pallas_call x5, Pallas kernels, call(): pl.pallas_call(with_copies, out_shape=jax.tree.unflatten(tree, [pltpu.VME...  16.4 us
    ppermute x15, waiting for transfers between devices, swap_pairs(): lax.ppermute(array, axis, [(i, paired(i, step, count)) for i in range(cou...  15.8 us
    all_to_all x1, waiting for transfers between devices, body(): got = lax.all_to_all(packed, ('z', 'x'), 0, 0, tiled=True)  12.8 us
    ppermute x15, starting transfers between devices, swap_pairs(): lax.ppermute(array, axis, [(i, paired(i, step, count)) for i in range(cou...  9.56 us
    all_to_all x1, starting transfers between devices, spread_rows(): return lax.all_to_all(copies, ('z', 'x'), 0, 0, tiled=True)  7.28 us
    all_to_all x1, starting transfers between devices, body(): got = lax.all_to_all(sent, ('z', 'x', 'tp'), 0, 0, tiled=True)  4.66 us
    all_to_all x1, waiting for transfers between devices, spread_rows(): return lax.all_to_all(copies, ('z', 'x'), 0, 0, tiled=True)  4.01 us
  transfers between devices with their start and end apart: 18, of which 7 were waited for; matrix products, arithmetic and copies ran while one was open for 5% of the time, Pallas kernels for 8%

profile of v2, /device:TPU:0, one launch (start us, length us, event | category | flops | bytes accessed | tf_op | source)
XLA Modules:
  0.0 105.5 jit_solution(1122473526019095702)
XLA Ops:
  0.0 1.5 %broadcast_in_dim.28 = bf16[8,16,1024]{2,1,0:T(8,128)(2,1)} broadcast(bf16[16,1024]{1,0:T(8,128)(2,1)} %param.21), dimensions={1,2} | broadcast | bytes 294912 | tf_op jit(solution)/shard_map/broadcast_in_dim | solution.py:39
  1.5 7.3 %all-to-all-start = ((bf16[8,16,1024]{2,1,0:T(8,128)(2,1)}), bf16[8,16,1024]{2,1,0:T(8,128)(2,1)S(1)}, u32[]{:S(2)}, u32[]{:S(2)}) async-start(bf16[8,16,1024]{2,1,0:T(8,128)(2,1)} %broadcast_in_dim.28), calls=%async_computation | async-start | bytes 524288 | tf_op jit(solution)/shard_map/all_to_all | solution.py:40
  9.9 1.4 %reshape.32.refs_4_ = f32[16,64]{1,0:T(8,128)} reshape(f32[1024]{0:T(1024)} %param.31) | data formatting | bytes 8192 | tf_op jit(solution)/shard_map/reshape | solution.py:531
  11.3 1.7 %shard_map.199 = (f32[1,1024]{1,0:T(1,128)S(1)}, f32[1,2048]{1,0:T(1,128)S(1)}, f32[4,2,1,128]{3,2,1,0:T(1,128)S(1)}, f32[4,2,1,128]{3,2,1,0:T(1,128)S(1)}, f32[...) custom-call(f32[1,1024]{1,0:T(1,128)} %bitcast.19, f32[1,2048]{1,0:T(1,128)} %bitcast.18, f32[4,2,1,128]{3,2,1,0:T(1,128)} %bitcast.20, ...), custom_call_target="tpu_custom_call" | custom-call | tf_op jit(solution)/shard_map/pallas_call | solution.py:107
  13.7 4.0 %all-to-all-done.refs_0_ = bf16[8,16,1024]{2,1,0:T(8,128)(2,1)S(1)} async-done(((bf16[8,16,1024]{2,1,0:T(8,128)(2,1)}), bf16[8,16,1024]{2,1,0:T(8,128)(2,1)S(1)}, u32[]{:S(2)}, u32[]{:S(2)}) %all-to-all-start) | async-done | bytes 262176 | tf_op jit(solution)/shard_map/all_to_all | solution.py:40
  17.7 4.2 %shard_map.200 = bf16[8,2,5,2,16,128]{5,4,3,2,1,0:T(8,128)(2,1)} custom-call(s32[5]{0:T(128)S(1)} %stack.19.place, bf16[8,16,1024]{2,1,0:T(8,128)(2,1)S(1)} %all-to-all-done.refs_0_, f32[1,1024]{1,0:T(1,128)S(1)} %get-tuple-element.13.refs_1_, bf16[1024,128]{1,0:T(8,128)(2,1)S(1)} %collective-permute-done.refs_2_, ...), custom_call_target="tpu_custom_call" | custom-call | tf_op jit(solution)/shard_map/pallas_call | solution.py:79
  21.9 4.7 %all-to-all-start.1 = ((bf16[16,5,2,16,128]{4,3,2,1,0:T(8,128)(2,1)}), bf16[16,5,2,16,128]{4,3,2,1,0:T(8,128)(2,1)S(1)}, u32[]{:S(2)}, u32[]{:S(2)}) async-start(bf16[16,5,2,16,128]{4,3,2,1,0:T(8,128)(2,1)} %bitcast.9), calls=%async_computation.1 | async-start | bytes 1310720 | tf_op jit(solution)/shard_map/all_to_all | solution.py:538
  26.6 1.9 %collective-permute-start.9 = (bf16[1024,128]{1,0:T(8,128)(2,1)}, bf16[1024,128]{1,0:T(8,128)(2,1)S(1)}, u32[]{:S(2)}, u32[]{:S(2)}) collective-permute-start(bf16[1024,128]{1,0:T(8,128)(2,1)} %refs_8_.4), channel_id=1, source_target_pairs={{0,4},{4,0},{1,5},{5,1},{2,6},{6,2},{3,7},{7,3},{8,12},{12,8},{9,1... | collective-permute-start | bytes 786440 | tf_op jit(solution)/shard_map/ppermute | solution.py:35
  30.4 9.8 %collective-permute-done.9.refs_6_ = bf16[1024,128]{1,0:T(8,128)(2,1)S(1)} collective-permute-done((bf16[1024,128]{1,0:T(8,128)(2,1)}, bf16[1024,128]{1,0:T(8,128)(2,1)S(1)}, u32[]{:S(2)}, u32[]{:S(2)}) %collective-permute-start.9) | collective-permute-done | bytes 262176 | tf_op jit(solution)/shard_map/ppermute | solution.py:35
  40.2 1.4 %select_reduce_fusion = f32[16,16]{1,0:T(8,128)} fusion(f32[16,6]{0,1:T(8,128)S(1)} %divide_multiply_fusion, s32[16,6]{0,1:T(8,128)} %param.34), kind=kLoop, calls=%fused_computation.2 | loop fusion | flops 4352 | bytes 1792 | tf_op jit(solution)/shard_map/reduce_sum | solution.py:552
  41.6 2.0 %all-to-all-done.1 = bf16[16,5,2,16,128]{4,3,2,1,0:T(8,128)(2,1)S(1)} async-done(((bf16[16,5,2,16,128]{4,3,2,1,0:T(8,128)(2,1)}), bf16[16,5,2,16,128]{4,3,2,1,0:T(8,128)(2,1)S(1)}, u32[]{:S(2)}, u32[]{:S(2)}) %all-to-all-start.1) | async-done | bytes 655392 | tf_op jit(solution)/shard_map/all_to_all | solution.py:538
  44.3 3.0 %shard_map.201.refs_1_ = bf16[16,1024]{1,0:T(8,128)(2,1)S(1)} custom-call(s32[5]{0:T(128)S(1)} %stack.19.place, bf16[8,2,5,2,16,128]{5,4,3,2,1,0:T(8,128)(2,1)S(1)} %bitcast.16, bf16[16,16,4096]{2,1,0:T(8,128)(2,1)S(1)} %get-tuple-element.14.refs_1_, f32[4,2,1,128]{3,2,1,0:T(1,128)S(1)} %get-tuple-element.15.refs_2_, f32[4,2,1,128]{3,2,1,0:T(1,128)S(1)} %copy-done.3, ...), custom_call_target="tpu_custom_call" | custom-call | tf_op jit(solution)/shard_map/pallas_call | solution.py:79
  47.3 1.8 %collective-permute-start.5 = (bf16[16,1024]{1,0:T(8,128)(2,1)S(1)}, bf16[16,1024]{1,0:T(8,128)(2,1)S(1)}, u32[]{:S(2)}, u32[]{:S(2)}) collective-permute-start(bf16[16,1024]{1,0:T(8,128)(2,1)S(1)} %shard_map.201.refs_1_), channel_id=1, source_target_pairs={{0,8},{8,0},{16,24},{24,16},{1,9},{9,1},{17,25},{25,17},{2,10},{10... | collective-permute-start | bytes 98312 | tf_op jit(solution)/shard_map/ppermute | solution.py:35
  50.0 1.8 %collective-permute-start.7 = (bf16[16,1024]{1,0:T(8,128)(2,1)S(1)}, bf16[16,1024]{1,0:T(8,128)(2,1)S(1)}, u32[]{:S(2)}, u32[]{:S(2)}) collective-permute-start(bf16[16,1024]{1,0:T(8,128)(2,1)S(1)} %shard_map.201.refs_1_), channel_id=1, source_target_pairs={{0,24},{8,16},{16,8},{24,0},{1,25},{9,17},{17,9},{25,1},{2,26},{10... | collective-permute-start | bytes 98312 | tf_op jit(solution)/shard_map/ppermute | solution.py:35
  52.5 1.5 %collective-permute-done.6.refs_3_ = bf16[16,1024]{1,0:T(8,128)(2,1)S(1)} collective-permute-done((bf16[16,1024]{1,0:T(8,128)(2,1)S(1)}, bf16[16,1024]{1,0:T(8,128)(2,1)S(1)}, u32[]{:S(2)}, u32[]{:S(2)}) %collective-permute-start.6) | collective-permute-done | bytes 32800 | tf_op jit(solution)/shard_map/ppermute | solution.py:35
  54.0 1.7 %collective-permute-done.7.refs_4_ = bf16[16,1024]{1,0:T(8,128)(2,1)S(1)} collective-permute-done((bf16[16,1024]{1,0:T(8,128)(2,1)S(1)}, bf16[16,1024]{1,0:T(8,128)(2,1)S(1)}, u32[]{:S(2)}, u32[]{:S(2)}) %collective-permute-start.7) | collective-permute-done | bytes 32800 | tf_op jit(solution)/shard_map/ppermute | solution.py:35
  55.7 2.2 %shard_map.202.refs_1_ = bf16[4,4,16,128]{3,2,1,0:T(8,128)(2,1)S(1)} custom-call(s32[5]{0:T(128)S(1)} %stack.19.place, bf16[8,16,1024]{2,1,0:T(8,128)(2,1)S(1)} %all-to-all-done.refs_0_, bf16[16,1024]{1,0:T(8,128)(2,1)S(1)} %shard_map.201.refs_1_, bf16[16,1024]{1,0:T(8,128)(2,1)S(1)} %collective-permute-done.5.refs_2_, ...), custom_call_target="tpu_custom_call" | custom-call | tf_op jit(solution)/shard_map/pallas_call | solution.py:79
  57.9 1.5 %collective-permute-start.11 = (bf16[4,4,16,128]{3,2,1,0:T(8,128)(2,1)S(1)}, bf16[4,4,16,128]{3,2,1,0:T(8,128)(2,1)S(1)}, u32[]{:S(2)}, u32[]{:S(2)}) collective-permute-start(bf16[4,4,16,128]{3,2,1,0:T(8,128)(2,1)S(1)} %shard_map.202.refs_1_), channel_id=1, source_target_pairs={{0,1},{1,0},{2,3},{3,2},{4,5},{5,4},{6,7},{7,6},{8,9},{9,8},{10,11... | collective-permute-start | bytes 196616 | tf_op jit(solution)/shard_map/ppermute | solution.py:35
  59.5 2.8 %collective-permute-done.11.refs_2_ = bf16[4,4,16,128]{3,2,1,0:T(8,128)(2,1)S(1)} collective-permute-done((bf16[4,4,16,128]{3,2,1,0:T(8,128)(2,1)S(1)}, bf16[4,4,16,128]{3,2,1,0:T(8,128)(2,1)S(1)}, u32[]{:S(2)}, u32[]{:S(2)}) %collective-permute-start.11) | collective-permute-done | bytes 65568 | tf_op jit(solution)/shard_map/ppermute | solution.py:35
  62.2 1.4 %shard_map.203 = bf16[8,17,16,128]{3,2,1,0:T(8,128)(2,1)} custom-call(s32[5]{0:T(128)S(1)} %stack.19.place, bf16[1,16,128]{2,1,0:T(8,128)(2,1)S(1)} %maximum_bitcast_fusion.refs_0_, bf16[4,4,16,128]{3,2,1,0:T(8,128)(2,1)S(1)} %shard_map.202.refs_1_, bf16[4,4,16,128]{3,2,1,0:T(8,128)(2,1)S(1)} %collective-permute-done.11.refs_2_), custom_call_target="tpu_custom_call" | custom-call | tf_op jit(solution)/shard_map/pallas_call | solution.py:79
  63.6 3.9 %all-to-all-start.2 = ((bf16[8,17,16,128]{3,2,1,0:T(8,128)(2,1)}), bf16[8,17,16,128]{3,2,1,0:T(8,128)(2,1)S(1)}, u32[]{:S(2)}, u32[]{:S(2)}) async-start(bf16[8,17,16,128]{3,2,1,0:T(8,128)(2,1)} %shard_map.203), calls=%async_computation.2 | async-start | bytes 1114112 | tf_op jit(solution)/shard_map/all_to_all | solution.py:560
  67.6 12.8 %all-to-all-done.2.refs_0_ = bf16[8,17,16,128]{3,2,1,0:T(8,128)(2,1)S(1)} async-done(((bf16[8,17,16,128]{3,2,1,0:T(8,128)(2,1)}), bf16[8,17,16,128]{3,2,1,0:T(8,128)(2,1)S(1)}, u32[]{:S(2)}, u32[]{:S(2)}) %all-to-all-start.2) | async-done | bytes 557088 | tf_op jit(solution)/shard_map/all_to_all | solution.py:560
  80.4 5.5 %shard_map.204 = (bf16[8,2,16,1024]{3,2,1,0:T(8,128)(2,1)S(1)}, bf16[16,1024]{1,0:T(8,128)(2,1)S(1)}) custom-call(s32[5]{0:T(128)S(1)} %stack.19.place, bf16[8,17,16,128]{3,2,1,0:T(8,128)(2,1)S(1)} %all-to-all-done.2.refs_0_, f32[1,2048]{1,0:T(1,128)S(1)} %copy-done.1, bf16[2048,256]{1,0:T(8,128)(2,1)} %bitcast.11.refs_2_, ...), custom_call_target="tpu_custom_call" | custom-call | tf_op jit(solution)/shard_map/pallas_call | solution.py:79
  86.0 18.8 %all_to_all.20 = bf16[16,16,1024]{2,1,0:T(8,128)(2,1)S(1)} all-to-all(bf16[16,16,1024]{2,1,0:T(8,128)(2,1)S(1)} %bitcast.17), channel_id=1, replica_groups=mesh['z'=4,'x'=2,'core'=2,'tp'=2] {'z','x','tp'}, dimensions={0} | all-to-all | bytes 1048576 | tf_op jit(solution)/shard_map/all_to_all | solution.py:569
  (41 shorter events, 6.7 us)
Async XLA Ops:
  1.5 16.2 %all-to-all-start = ((bf16[8,16,1024]{2,1,0:T(8,128)(2,1)}), bf16[8,16,1024]{2,1,0:T(8,128)(2,1)S(1)}, u32[]{:S(2)}, u32[]{:S(2)}) async-start(bf16[8,16,1024]{2,1,0:T(8,128)(2,1)} %broadcast_in_dim.28), calls=%async_computation | async-start | bytes 524288 | tf_op jit(solution)/shard_map/all_to_all | solution.py:40
  8.8 4.9 %collective-permute-start = (bf16[1024,128]{1,0:T(8,128)(2,1)}, bf16[1024,128]{1,0:T(8,128)(2,1)S(1)}, u32[]{:S(2)}, u32[]{:S(2)}) collective-permute-start(bf16[1024,128]{1,0:T(8,128)(2,1)} %refs_7_.1), channel_id=1, source_target_pairs={{0,2},{2,0},{1,3},{3,1},{4,6},{6,4},{5,7},{7,5},{8,10},{10,8},{9,1... | collective-permute-start | bytes 786440 | tf_op jit(solution)/shard_map/ppermute | solution.py:35
  8.8 4.9 %collective-permute-start.1 = (bf16[1024,128]{1,0:T(8,128)(2,1)}, bf16[1024,128]{1,0:T(8,128)(2,1)S(1)}, u32[]{:S(2)}, u32[]{:S(2)}) collective-permute-start(bf16[1024,128]{1,0:T(8,128)(2,1)} %refs_8_.3), channel_id=1, source_target_pairs={{0,2},{2,0},{1,3},{3,1},{4,6},{6,4},{5,7},{7,5},{8,10},{10,8},{9,1... | collective-permute-start | bytes 786440 | tf_op jit(solution)/shard_map/ppermute | solution.py:35
  9.3 4.4 %collective-permute-start.2 = (bf16[1024,128]{1,0:T(8,128)(2,1)}, bf16[1024,128]{1,0:T(8,128)(2,1)S(1)}, u32[]{:S(2)}, u32[]{:S(2)}) collective-permute-start(bf16[1024,128]{1,0:T(8,128)(2,1)} %refs_9_.2), channel_id=1, source_target_pairs={{0,2},{2,0},{1,3},{3,1},{4,6},{6,4},{5,7},{7,5},{8,10},{10,8},{9,1... | collective-permute-start | bytes 786440 | tf_op jit(solution)/shard_map/ppermute | solution.py:35
  9.4 4.3 %collective-permute-start.3 = (bf16[1024,128]{1,0:T(8,128)(2,1)}, bf16[1024,128]{1,0:T(8,128)(2,1)S(1)}, u32[]{:S(2)}, u32[]{:S(2)}) collective-permute-start(bf16[1024,128]{1,0:T(8,128)(2,1)} %refs_10_.2), channel_id=1, source_target_pairs={{0,2},{2,0},{1,3},{3,1},{4,6},{6,4},{5,7},{7,5},{8,10},{10,8},{9,1... | collective-permute-start | bytes 786440 | tf_op jit(solution)/shard_map/ppermute | solution.py:35
  9.8 3.9 %collective-permute-start.4 = (bf16[1024,128]{1,0:T(8,128)(2,1)}, bf16[1024,128]{1,0:T(8,128)(2,1)}, u32[]{:S(2)}, u32[]{:S(2)}) collective-permute-start(bf16[1024,128]{1,0:T(8,128)(2,1)} %refs_11_.1), channel_id=1, source_target_pairs={{0,2},{2,0},{1,3},{3,1},{4,6},{6,4},{5,7},{7,5},{8,10},{10,8},{9,1... | collective-permute-start | bytes 786440 | tf_op jit(solution)/shard_map/ppermute | solution.py:35
  13.0 0.6 copy-start
  13.6 8.3 %copy-start.2 = (f32[4,2,1,128]{3,2,1,0:T(1,128)}, f32[4,2,1,128]{3,2,1,0:T(1,128)S(1)}, u32[]{:S(2)}) copy-start(f32[4,2,1,128]{3,2,1,0:T(1,128)S(1)} %get-tuple-element.16.refs_3_) | copy-start | bytes 12292
  21.9 21.7 %all-to-all-start.1 = ((bf16[16,5,2,16,128]{4,3,2,1,0:T(8,128)(2,1)}), bf16[16,5,2,16,128]{4,3,2,1,0:T(8,128)(2,1)S(1)}, u32[]{:S(2)}, u32[]{:S(2)}) async-start(bf16[16,5,2,16,128]{4,3,2,1,0:T(8,128)(2,1)} %bitcast.9), calls=%async_computation.1 | async-start | bytes 1310720 | tf_op jit(solution)/shard_map/all_to_all | solution.py:538
  26.6 13.7 %collective-permute-start.9 = (bf16[1024,128]{1,0:T(8,128)(2,1)}, bf16[1024,128]{1,0:T(8,128)(2,1)S(1)}, u32[]{:S(2)}, u32[]{:S(2)}) collective-permute-start(bf16[1024,128]{1,0:T(8,128)(2,1)} %refs_8_.4), channel_id=1, source_target_pairs={{0,4},{4,0},{1,5},{5,1},{2,6},{6,2},{3,7},{7,3},{8,12},{12,8},{9,1... | collective-permute-start | bytes 786440 | tf_op jit(solution)/shard_map/ppermute | solution.py:35
  28.5 23.4 %collective-permute-start.8 = (bf16[1024,128]{1,0:T(8,128)(2,1)}, bf16[1024,128]{1,0:T(8,128)(2,1)S(1)}, u32[]{:S(2)}, u32[]{:S(2)}) collective-permute-start(bf16[1024,128]{1,0:T(8,128)(2,1)} %refs_8_.4), channel_id=1, source_target_pairs={{0,2},{2,0},{1,3},{3,1},{4,6},{6,4},{5,7},{7,5},{8,10},{10,8},{9,1... | collective-permute-start | bytes 786440 | tf_op jit(solution)/shard_map/ppermute | solution.py:35
  40.2 11.7 %collective-permute-start.10 = (bf16[1024,128]{1,0:T(8,128)(2,1)S(1)}, bf16[1024,128]{1,0:T(8,128)(2,1)}, u32[]{:S(2)}, u32[]{:S(2)}) collective-permute-start(bf16[1024,128]{1,0:T(8,128)(2,1)S(1)} %collective-permute-done.9.refs_6_), channel_id=1, source_target_pairs={{0,2},{2,0},{1,3},{3,1},{4,6},{6,4},{5,7},{7,5},{8,10},{10,8},{9,1... | collective-permute-start | bytes 786440 | tf_op jit(solution)/shard_map/ppermute | solution.py:35
  43.6 8.2 %copy-start.4 = (f32[16,16]{1,0:T(8,128)S(1)}, f32[16,16]{1,0:T(8,128)}, u32[]{:S(2)}) copy-start(f32[16,16]{1,0:T(8,128)} %select_reduce_fusion) | copy-start | bytes 3076
  43.6 0.7 copy-start.3
  47.3 33.1 %copy-start.1 = (f32[1,2048]{1,0:T(1,128)S(1)}, f32[1,2048]{1,0:T(1,128)}, u32[]{:S(2)}) copy-start(f32[1,2048]{1,0:T(1,128)} %copy-done) | copy-start | bytes 24580
  47.3 5.1 %collective-permute-start.5 = (bf16[16,1024]{1,0:T(8,128)(2,1)S(1)}, bf16[16,1024]{1,0:T(8,128)(2,1)S(1)}, u32[]{:S(2)}, u32[]{:S(2)}) collective-permute-start(bf16[16,1024]{1,0:T(8,128)(2,1)S(1)} %shard_map.201.refs_1_), channel_id=1, source_target_pairs={{0,8},{8,0},{16,24},{24,16},{1,9},{9,1},{17,25},{25,17},{2,10},{10... | collective-permute-start | bytes 98312 | tf_op jit(solution)/shard_map/ppermute | solution.py:35
  49.1 4.9 %collective-permute-start.6 = (bf16[16,1024]{1,0:T(8,128)(2,1)S(1)}, bf16[16,1024]{1,0:T(8,128)(2,1)S(1)}, u32[]{:S(2)}, u32[]{:S(2)}) collective-permute-start(bf16[16,1024]{1,0:T(8,128)(2,1)S(1)} %shard_map.201.refs_1_), channel_id=1, source_target_pairs={{0,16},{8,24},{16,0},{24,8},{1,17},{9,25},{17,1},{25,9},{2,18},{10... | collective-permute-start | bytes 98312 | tf_op jit(solution)/shard_map/ppermute | solution.py:35
  50.0 5.7 %collective-permute-start.7 = (bf16[16,1024]{1,0:T(8,128)(2,1)S(1)}, bf16[16,1024]{1,0:T(8,128)(2,1)S(1)}, u32[]{:S(2)}, u32[]{:S(2)}) collective-permute-start(bf16[16,1024]{1,0:T(8,128)(2,1)S(1)} %shard_map.201.refs_1_), channel_id=1, source_target_pairs={{0,24},{8,16},{16,8},{24,0},{1,25},{9,17},{17,9},{25,1},{2,26},{10... | collective-permute-start | bytes 98312 | tf_op jit(solution)/shard_map/ppermute | solution.py:35
  51.9 15.7 %collective-permute-start.12 = (bf16[2048,256]{1,0:T(8,128)(2,1)}, bf16[2048,256]{1,0:T(8,128)(2,1)S(1)}, u32[]{:S(2)}, u32[]{:S(2)}) collective-permute-start(bf16[2048,256]{1,0:T(8,128)(2,1)} %bitcast.11.refs_2_), channel_id=1, source_target_pairs={{0,2},{2,0},{1,3},{3,1},{4,6},{6,4},{5,7},{7,5},{8,10},{10,8},{9,1... | collective-permute-start | bytes 3145736 | tf_op jit(solution)/shard_map/ppermute | solution.py:35
  51.9 15.7 %collective-permute-start.13 = (bf16[2048,256]{1,0:T(8,128)(2,1)}, bf16[2048,256]{1,0:T(8,128)(2,1)S(1)}, u32[]{:S(2)}, u32[]{:S(2)}) collective-permute-start(bf16[2048,256]{1,0:T(8,128)(2,1)} %bitcast.12.refs_3_), channel_id=1, source_target_pairs={{0,2},{2,0},{1,3},{3,1},{4,6},{6,4},{5,7},{7,5},{8,10},{10,8},{9,1... | collective-permute-start | bytes 3145736 | tf_op jit(solution)/shard_map/ppermute | solution.py:35
  52.4 15.2 %collective-permute-start.14 = (bf16[256,2048]{1,0:T(8,128)(2,1)}, bf16[256,2048]{1,0:T(8,128)(2,1)}, u32[]{:S(2)}, u32[]{:S(2)}) collective-permute-start(bf16[256,2048]{1,0:T(8,128)(2,1)} %bitcast.13.refs_4_), channel_id=1, source_target_pairs={{0,2},{2,0},{1,3},{3,1},{4,6},{6,4},{5,7},{7,5},{8,10},{10,8},{9,1... | collective-permute-start | bytes 3145736 | tf_op jit(solution)/shard_map/ppermute | solution.py:35
  57.9 4.3 %collective-permute-start.11 = (bf16[4,4,16,128]{3,2,1,0:T(8,128)(2,1)S(1)}, bf16[4,4,16,128]{3,2,1,0:T(8,128)(2,1)S(1)}, u32[]{:S(2)}, u32[]{:S(2)}) collective-permute-start(bf16[4,4,16,128]{3,2,1,0:T(8,128)(2,1)S(1)} %shard_map.202.refs_1_), channel_id=1, source_target_pairs={{0,1},{1,0},{2,3},{3,2},{4,5},{5,4},{6,7},{7,6},{8,9},{9,8},{10,11... | collective-permute-start | bytes 196616 | tf_op jit(solution)/shard_map/ppermute | solution.py:35
  63.6 16.8 %all-to-all-start.2 = ((bf16[8,17,16,128]{3,2,1,0:T(8,128)(2,1)}), bf16[8,17,16,128]{3,2,1,0:T(8,128)(2,1)S(1)}, u32[]{:S(2)}, u32[]{:S(2)}) async-start(bf16[8,17,16,128]{3,2,1,0:T(8,128)(2,1)} %shard_map.203), calls=%async_computation.2 | async-start | bytes 1114112 | tf_op jit(solution)/shard_map/all_to_all | solution.py:560

commit v3 on v2

--- a/solution.py
+++ b/solution.py
@@ -33,6 +33,11 @@
 def swap_pairs(array, axis, step):
     count = lax.axis_size(axis)
     return lax.ppermute(array, axis, [(i, paired(i, step, count)) for i in range(count)])
+
+
+def swap_chips(array, step, chips):
+    order = [(i, paired(i, step, chips)) for i in range(chips)]
+    return lax.ppermute(array, ("z", "x"), order)
 
 
 def spread_rows(rows):
@@ -114,61 +119,75 @@
     )(*(pltpu.with_memory_space_constraint(array, pltpu.HBM) for array in arrays))
 
 
-def square_holder(target, tp, chips_tp):
-    return (target + 1) % tp * chips_tp
-
-
-def project_kernel(sizes, place, rows, gain, *refs):
-    tp, chips_tp, roles = sizes
+def project_kernel(place, rows, gain, *refs):
+    roles = (len(refs) - 1) // 2
     other, own, out = refs[:roles], refs[roles : 2 * roles], refs[2 * roles]
     core = place[2]
     chips, seqs, part = rows.shape
     cols = own[0].shape[1]
-    chip = place[0] * place[4] + place[1]
-    group = chip // chips_tp
-    count = chips * seqs
-    left = rows[...].astype(F32).reshape(count, part)
-    square = jnp.sum(left * left, axis=1, keepdims=True)
-    high = square.astype(BF16)
-    low = (square - high.astype(F32)).astype(BF16)
-    scaled = (left * gain[...]).astype(BF16)
-    for shift in range(1, tp):
-        target = (group + shift) % tp
-        for index, vals in enumerate((high, low)):
-            vals = jnp.broadcast_to(vals.astype(F32), (count, cols)).astype(BF16)
-            out[:, target, 0, index] = vals.reshape(chips, seqs, cols)
-    for role in range(roles):
-        weight = jnp.concatenate((own[role][...], other[role][...]), axis=1)
+    scaled = (rows[...].astype(F32) * gain[...]).reshape(chips * seqs, part).astype(BF16)
+    order = [(role, 1 - core, other[role]) for role in range(roles)]
+    order += [(role, core, own[role]) for role in range(roles)]
+    for first in range(0, 2 * roles, 2):
+        pair = order[first : first + 2]
+        weight = jnp.concatenate([ref[...] for _, _, ref in pair], axis=1)
         product = dot(scaled, weight).astype(BF16).reshape(chips, seqs, 2 * cols)
-        out[:, group, role, core] = product[:, :, :cols]
-        out[:, group, role, 1 - core] = product[:, :, cols:]
-
-
-def project(kernels, place, rows, gain, own, other, tp):
+        for index, (role, side, _) in enumerate(pair):
+            out[:, role, side] = product[:, :, index * cols : (index + 1) * cols]
+
+
+def project(kernels, place, rows, gain, own, other):
     chips, seqs, part = rows.shape
     cols = own[0].shape[1]
     roles = len(own)
-    chips_tp = chips // tp
-    shape = (chips, tp, roles, 2, seqs, cols)
-    if kernels:
-        kernel = functools.partial(project_kernel, (tp, chips_tp, roles))
-        out = jax.ShapeDtypeStruct(shape, BF16)
-        return call(kernel, out, place, rows, gain, *other, late=own)
-    core = place[2]
-    group = (place[0] * place[4] + place[1]) // chips_tp
+    if kernels:
+        out = jax.ShapeDtypeStruct((chips, roles, 2, seqs, cols), BF16)
+        return call(project_kernel, out, place, rows, gain, *other, late=own)
     scaled = (rows.astype(F32) * gain[0]).astype(BF16).reshape(chips * seqs, part)
     pairs = []
     for mine, theirs in zip(own, other):
         sides = jnp.stack((dot(scaled, mine), dot(scaled, theirs))).astype(BF16)
-        pairs.append(jnp.where(core == 0, sides, sides[::-1]))
-    product = jnp.stack(pairs).reshape(roles, 2, chips, seqs, cols).transpose(2, 0, 1, 3, 4)
-    square = jnp.sum(jnp.square(rows.astype(F32)), axis=2)
+        pairs.append(jnp.where(place[2] == 0, sides, sides[::-1]))
+    product = jnp.stack(pairs).reshape(roles, 2, chips, seqs, cols)
+    return product.transpose(2, 0, 1, 3, 4)
+
+
+def square_of(tokens):
+    vals = tokens.astype(F32)
+    return jnp.sum(vals * vals, axis=1, keepdims=True)
+
+
+def pick_kernel(place, got, tokens, *outs):
+    chips, roles, sides, seqs, cols = got.shape
+    chips_tp = chips // (len(outs) + 1)
+    count = chips_tp * roles * sides
+    square = square_of(tokens[...])
+    high = square.astype(BF16).astype(F32)
+    for step, out in enumerate(outs):
+        target = paired(place[3], step + 1, len(outs) + 1)
+        block = got[pl.ds(target * chips_tp, chips_tp)]
+        out[:count] = block.reshape(count, seqs, cols)
+        out[count] = jnp.broadcast_to(high, (seqs, cols)).astype(BF16)
+        out[count + 1] = jnp.broadcast_to(square - high, (seqs, cols)).astype(BF16)
+
+
+def pick(kernels, place, got, tokens, tp):
+    chips, roles, sides, seqs, cols = got.shape
+    chips_tp = chips // tp
+    count = chips_tp * roles * sides
+    if kernels:
+        outs = [jax.ShapeDtypeStruct((count + 2, seqs, cols), BF16)] * (tp - 1)
+        return call(pick_kernel, outs, place, got, tokens)
+    square = square_of(tokens)
     high = square.astype(BF16)
-    low = (square - high.astype(F32)).astype(BF16)
-    marks = jnp.stack((high, low), axis=1)[:, None, :, :, None]
-    marks = jnp.broadcast_to(marks, (chips, roles, 2, seqs, cols))
-    here = (jnp.arange(tp) == group)[None, :, None, None, None, None]
-    return jnp.where(here, product[:, None], marks[:, None])
+    marks = jnp.stack((high, (square - high.astype(F32)).astype(BF16)))
+    marks = jnp.broadcast_to(marks, (2, seqs, cols))
+    outs = []
+    for step in range(1, tp):
+        start = paired(place[3], step, tp) * chips_tp
+        block = lax.dynamic_slice_in_dim(got, start, chips_tp, 0)
+        outs.append(jnp.concatenate((block.reshape(count, seqs, cols), marks), axis=0))
+    return outs
 
 
 def gates(decay_pre, rate_pre):
@@ -176,31 +195,31 @@
     return decay_rate, jax.nn.sigmoid(rate_pre)
 
 
-def mixer_kernel(place, got, state, decay_base, rate_base, head_gain, out, products, flat):
-    chips, tp, _, _, seqs, cols = got.shape
+def mixer_kernel(place, got, tokens, state, *refs):
+    *parts, decay_base, rate_base, head_gain, out, products, flat = refs
+    chips, roles, sides, seqs, cols = got.shape
+    tp = len(parts) + 1
     chips_tp = chips // tp
     heads = state.shape[1]
     count = seqs * heads
     half = count // 2
-    shard = place[3]
-    holder = square_holder(shard, tp, chips_tp)
-    square = jnp.zeros((seqs, cols), F32)
-    for source in range(tp):
-        for index in range(2):
-            square = square + got[holder, source, 0, index].astype(F32)
+    blocks = chips_tp * roles * sides
+    square = square_of(tokens[...])
+    for part in parts:
+        square = square + part[blocks].astype(F32) + part[blocks + 1].astype(F32)
     factor = lax.rsqrt(square / (heads * HEAD * tp) + RMS_EPS)
+    others = [part[:blocks].reshape(chips_tp, roles, sides, seqs, cols) for part in parts]
 
     def role(index, base=None):
-        vals = jnp.zeros((chips_tp, 2, seqs, cols), F32)
-        for source in range(tp):
-            vals = vals + got[pl.ds(shard * chips_tp, chips_tp), source, index].astype(F32)
+        vals = got[pl.ds(place[3] * chips_tp, chips_tp), index].astype(F32)
+        for other in others:
+            vals = vals + other[:, index].astype(F32)
         vals = vals * factor
         if base is not None:
             vals = vals + base[...]
         return vals.reshape(half, LANES)
 
     receptance, key_vec, value_vec = role(0), role(1), role(2)
-    decay_rate, in_rate = gates(role(3, decay_base), role(4, rate_base))
     row = lax.broadcasted_iota(jnp.int32, (LANES, LANES), 0)
     lane = lax.broadcasted_iota(jnp.int32, (LANES, LANES), 1)
     same_head = (row // HEAD == lane // HEAD).astype(F32)
@@ -211,6 +230,7 @@
         )
 
     unit_key = key_vec * lax.rsqrt(head_sum(key_vec * key_vec) + KEY_EPS)
+    decay_rate, in_rate = gates(role(3, decay_base), role(4, rate_base))
     steer = in_rate * receptance
     down_by = head_sum(unit_key * steer)
     raised = value_vec * head_sum(key_vec * steer)
@@ -258,9 +278,10 @@
         )
 
 
-def mixer(kernels, place, got, state, decay_base, rate_base, head_gain):
+def mixer(kernels, place, got, tokens, state, parts, decay_base, rate_base, head_gain):
     seqs, heads, _ = state.shape
-    chips, tp, roles, _, _, cols = got.shape
+    chips, roles, sides, _, cols = got.shape
+    tp = len(parts) + 1
     chips_tp = chips // tp
     part = heads * HEAD
     if kernels:
@@ -269,21 +290,21 @@
             jax.ShapeDtypeStruct((seqs, part), BF16),
             place,
             got,
+            tokens,
             state,
-            decay_base,
-            rate_base,
-            head_gain,
+            *parts,
             scratch=(
                 pltpu.VMEM((2 * seqs * heads, HEAD * HEAD), BF16),
                 pltpu.VMEM((seqs * heads, HEAD), F32),
             ),
+            late=(decay_base, rate_base, head_gain),
         )
-    shard = place[3]
-    holder = square_holder(shard, tp, chips_tp)
-    square = lax.dynamic_index_in_dim(got, holder, 0, keepdims=False)[:, 0].astype(F32)
-    factor = lax.rsqrt(jnp.sum(square, axis=(0, 1))[:, :1] / (part * tp) + RMS_EPS)
-    total = lax.dynamic_slice_in_dim(got, shard * chips_tp, chips_tp, 0)
-    total = jnp.sum(total.astype(F32), axis=1) * factor
+    square = square_of(tokens) + sum(other[-2:].astype(F32).sum(0)[:, :1] for other in parts)
+    factor = lax.rsqrt(square / (part * tp) + RMS_EPS)
+    total = lax.dynamic_slice_in_dim(got, place[3] * chips_tp, chips_tp, 0).astype(F32)
+    for other in parts:
+        total = total + other[:-2].astype(F32).reshape(total.shape)
+    total = total * factor
     total = total.transpose(1, 3, 0, 2, 4).reshape(roles, seqs, part)
 
     def per_head(vals):
@@ -359,28 +380,31 @@
     for line in range(lines):
         for slot in range(slots):
             vals = sum(part[line, slot].astype(F32) for part in parts).astype(BF16)
-            for chip in range(out.shape[0]):
-                out[chip, line * slots + slot] = vals
+            out[line * slots + slot] = vals
     for index in range(tables.shape[0]):
-        for chip in range(out.shape[0]):
-            out[chip, lines * slots + index] = tables[index]
-
-
-def residual(kernels, place, parts, tables, chips):
+        out[lines * slots + index] = tables[index]
+
+
+def residual(kernels, place, parts, tables):
     lines, slots, seqs, cols = parts[0].shape
     tiles = lines * slots + tables.shape[0]
     if kernels:
-        shape = jax.ShapeDtypeStruct((chips, tiles, seqs, cols), BF16)
+        shape = jax.ShapeDtypeStruct((tiles, seqs, cols), BF16)
         return call(residual_kernel, shape, place, tables, *parts)
     total = sum(part.astype(F32) for part in parts).astype(BF16)
-    total = jnp.concatenate((total.reshape(lines * slots, seqs, cols), tables), axis=0)
-    return jnp.broadcast_to(total[None], (chips,) + total.shape)
-
-
-def expert_kernel(sizes, place, got, gain, *refs):
+    return jnp.concatenate((total.reshape(lines * slots, seqs, cols), tables), axis=0)
+
+
+def expert_kernel(sizes, place, *refs):
     x_size, experts = sizes
-    own, other, shared = refs[:3], refs[3:6], refs[6:9]
-    out, resid, left, home = refs[9:]
+    *refs, left, got = refs
+    chips = got.shape[0]
+    chip = place[0] * x_size + place[1]
+    for step in range(chips):
+        got[paired(chip, step, chips)] = refs[step][...]
+    gain, *refs = refs[chips:]
+    own, other = (refs[0], refs[1], refs[4]), (refs[2], refs[3], refs[5])
+    out, resid, home = refs[6:]
     chips, tp, seqs, part = out.shape
     z_size = chips // x_size
     cols = got.shape[3]
@@ -388,7 +412,6 @@
     width = part * tp
     count = chips * seqs
     z, x, core, shard = (place[index] for index in range(4))
-    chip = z * x_size + x
     for index in range(chips):
         z_to, x_from = divmod(index, x_size)
         square = jnp.zeros((seqs, cols), F32)
@@ -426,21 +449,19 @@
 
     own_hidden = scaled(own, chip * 2 + core)
     other_hidden = scaled(other, chip * 2 + 1 - core)
-    home_hidden = hidden_of(left[chip], shared).astype(BF16)
+    home[...] = left[chip]
     for target in range(tp):
         for start in range(0, part, 512):
             lanes = slice(start, min(start + 512, part))
             span = slice(target * part + lanes.start, target * part + lanes.stop)
             vals = dot(own_hidden, own[2][:, span]) + dot(other_hidden, other[2][:, span])
             vals = vals.reshape(chips, seqs, lanes.stop - lanes.start)
-            home[...] = dot(home_hidden, shared[2][:, span])
-            for index in range(chips):
-                extra = jnp.where(chip == index, home[...], 0.0)
-                out[index, target, :, lanes] = (vals[index] + extra).astype(BF16)
-
-
-def expert_rows(kernels, place, got, gain, own, other, shared, tp, x_size):
-    chips, _, seqs, cols = got.shape
+            out[:, target, :, lanes] = vals.astype(BF16)
+
+
+def expert_rows(kernels, place, got, gain, own, other, tp, x_size):
+    chips = len(got) if kernels else got.shape[0]
+    seqs, cols = got[0].shape[-2:]
     z_size = chips // x_size
     width = gain.shape[1]
     slots = width // (z_size * cols)
@@ -451,10 +472,15 @@
         shapes = [
             jax.ShapeDtypeStruct((chips, tp, seqs, part), BF16),
             jax.ShapeDtypeStruct((seqs, part), BF16),
+            jax.ShapeDtypeStruct((seqs, width), BF16),
         ]
-        scratch = (pltpu.VMEM((chips, seqs, width), BF16), pltpu.VMEM((seqs, 512), F32))
+        scratch = (
+            pltpu.VMEM((chips, seqs, width), BF16),
+            pltpu.VMEM((chips,) + got[0].shape, BF16),
+        )
+        later = other[:2] + (own[2], other[2])
         return call(
-            kernel, shapes, place, got, gain, *own, *other, scratch=scratch, late=shared
+            kernel, shapes, place, *got, gain, *own[:2], scratch=scratch, late=later
         )
     chip = place[0] * place[4] + place[1]
     rows = got[:, : z_size * slots].reshape(z_size, x_size, z_size, slots, seqs, cols)
@@ -479,11 +505,35 @@
 
     routed = product(own, chip * 2 + place[2]) + product(other, chip * 2 + 1 - place[2])
     home = lax.dynamic_index_in_dim(rows, chip, 0, keepdims=False)
-    home = dot(hidden_of(home, shared).astype(BF16), shared[2])
-    here = jnp.arange(chips)[:, None, None] == chip
-    routed = routed.reshape(chips, seqs, width) + jnp.where(here, home[None], 0.0)
     routed = routed.astype(BF16).reshape(chips, seqs, tp, part).transpose(0, 2, 1, 3)
-    return routed, resid
+    return routed, resid, home
+
+
+def shared_kernel(place, home, gate, up, down, *refs):
+    *outs, whole = refs
+    tp, seqs, part = whole.shape
+    hidden = jax.nn.silu(dot(home[...], gate[...])) * dot(home[...], up[...])
+    hidden = hidden.astype(BF16)
+    for target in range(tp):
+        whole[target] = dot(hidden, down[:, target * part : (target + 1) * part]).astype(BF16)
+    for step, out in enumerate(outs):
+        out[...] = whole[paired(place[3], step, tp)]
+
+
+def shared_rows(kernels, place, home, weights, tp):
+    seqs, width = home.shape
+    part = width // tp
+    if kernels:
+        outs = [jax.ShapeDtypeStruct((seqs, part), BF16)] * tp
+        scratch = (pltpu.VMEM((tp, seqs, part), BF16),)
+        return call(shared_kernel, outs, place, home, *weights, scratch=scratch)
+    gate, up, down = weights
+    hidden = (jax.nn.silu(dot(home, gate)) * dot(home, up)).astype(BF16)
+    whole = dot(hidden, down).astype(BF16)
+    return [
+        lax.dynamic_slice_in_dim(whole, paired(place[3], step, tp) * part, part, 1)
+        for step in range(tp)
+    ]
 
 
 def body(
@@ -530,14 +580,14 @@
     decay_base, rate_base = decay_base.reshape(blocks), rate_base.reshape(blocks)
     head_gain = head_gain.reshape(part // HEAD, HEAD)
     if kernels:
-        mix_gain, moe_gain, decay_base, rate_base, head_gain, state = fetch(
-            mix_gain, moe_gain, decay_base, rate_base, head_gain, state
-        )
-    sent = project(kernels, place, rows, mix_gain, own_w, other_w, tp)
-    sent = sent.reshape((chips * tp,) + sent.shape[2:])
-    got = lax.all_to_all(sent, ("z", "x", "tp"), 0, 0, tiled=True)
-    got = got.reshape((chips, tp) + got.shape[1:])
-    mixed = mixer(kernels, place, got, state, decay_base, rate_base, head_gain)
+        mix_gain, moe_gain, state = fetch(mix_gain, moe_gain, state)
+    sent = project(kernels, place, rows, mix_gain, own_w, other_w)
+    got = lax.all_to_all(sent, ("z", "x"), 0, 0, tiled=True)
+    parts = pick(kernels, place, got, tokens, tp)
+    parts = [swap_pairs(part_sum, "tp", index + 1) for index, part_sum in enumerate(parts)]
+    mixed = mixer(
+        kernels, place, got, tokens, state, parts, decay_base, rate_base, head_gain
+    )
 
     out_w = []
     for step in range(x_size):
@@ -556,18 +606,21 @@
     pad = jnp.zeros((seqs, -(2 * experts) % lanes), BF16)
     tables = jnp.concatenate((high, low, pad), axis=1)
     tables = tables.reshape(seqs, -1, lanes).transpose(1, 0, 2)
-    packed = residual(kernels, place, partials, tables, chips)
-    got = lax.all_to_all(packed, ("z", "x"), 0, 0, tiled=True)
+    packed = residual(kernels, place, partials, tables)
+    if kernels:
+        got = [packed] + [swap_chips(packed, step, chips) for step in range(1, chips)]
+    else:
+        got = spread_rows(packed)
 
     own = (expert_gate[0], expert_up[0], expert_down[0])
     other = tuple(swap_pairs(weight, "core", 1) for weight in own)
-    shared = (shared_gate, shared_up, shared_down)
-    routed, resid = expert_rows(
-        kernels, place, got, moe_gain, own, other, shared, tp, x_size
-    )
+    routed, resid, home = expert_rows(kernels, place, got, moe_gain, own, other, tp, x_size)
     routed = routed.reshape(chips * tp, seqs, part)
     returned = lax.all_to_all(routed, ("z", "x", "tp"), 0, 0, tiled=True)
-    return (resid.astype(F32) + jnp.sum(returned.astype(F32), axis=0)).astype(BF16)
+    added = shared_rows(kernels, place, home, (shared_gate, shared_up, shared_down), tp)
+    added = [added[0]] + [swap_pairs(added[step], "tp", step) for step in range(1, tp)]
+    total = resid.astype(F32) + sum(piece.astype(F32) for piece in added)
+    return (total + jnp.sum(returned.astype(F32), axis=0)).astype(BF16)
 
 
 def solution(mesh):

time: 106 us -> 100 us (0.943)
  blocking collectives: 18.8 us -> 0 us
  starting transfers between devices: 25.5 us -> 38.2 us
  waiting for transfers between devices: 34.6 us -> 38.5 us
  other arithmetic: 4.07 us -> 1.96 us
  local copies, waits for them, and re-layouts: 4.28 us -> 3.16 us
    all_to_all x1 -> x0, blocking collectives: 18.8 us -> none  [body(): returned = lax.all_to_all(routed, ('z', 'x', 'tp'), 0, 0, tiled=True)]
    ppermute x0 -> x7, starting transfers between devices: none -> 11.2 us  [swap_chips(): return lax.ppermute(array, ('z', 'x'), order)]
    ppermute x0 -> x7, waiting for transfers between devices: none -> 4.88 us  [swap_chips(): return lax.ppermute(array, ('z', 'x'), order)]
    ppermute x15 -> x17, waiting for transfers between devices: 15.8 us -> 13 us  [swap_pairs(): lax.ppermute(array, axis, [(i, paired(i, step, count)) for i in range(cou...]
    ppermute x15 -> x17, starting transfers between devices: 9.56 us -> 11.6 us  [swap_pairs(): lax.ppermute(array, axis, [(i, paired(i, step, count)) for i in range(cou...]
    all_to_all x1, waiting for transfers between devices: 4.01 us -> 5.54 us  [spread_rows(): return lax.all_to_all(copies, ('z', 'x'), 0, 0, tiled=True)]
    reduce_sum x1, other arithmetic: 1.38 us -> 0.09 us  [body(): table = jnp.sum(jnp.where(hit, share[:, :, None], 0.0), axis=1)]
    reduce_sum x1, other arithmetic: 1.21 us -> 0.02 us  [body(): jnp.sum(route_weight, axis=1, keepdims=True)]
  transfers between devices with their start and end apart: 18 -> 27, of which waited for: 7 -> 11; matrix products, arithmetic and copies ran while one was open for 5% -> 2% of each run, Pallas kernels for 8% -> 10%
where the time goes in v3:
time: 100 us; the launch traced here: 99.6 us
  waiting for transfers between devices  38.5 us (38%)
  starting transfers between devices  38.2 us (38%)
  Pallas kernels  17.5 us (18%)
  local copies, waits for them, and re-layouts  3.16 us (3%)
  other arithmetic  1.96 us (2%)
    pallas_call x7, Pallas kernels, call(): pl.pallas_call(with_copies, out_shape=jax.tree.unflatten(tree, [pltpu.VME...  15.8 us
    ppermute x17, waiting for transfers between devices, swap_pairs(): lax.ppermute(array, axis, [(i, paired(i, step, count)) for i in range(cou...  13 us
    ppermute x17, starting transfers between devices, swap_pairs(): lax.ppermute(array, axis, [(i, paired(i, step, count)) for i in range(cou...  11.6 us
    ppermute x7, starting transfers between devices, swap_chips(): return lax.ppermute(array, ('z', 'x'), order)  11.2 us
    all_to_all x1, waiting for transfers between devices, body(): returned = lax.all_to_all(routed, ('z', 'x', 'tp'), 0, 0, tiled=True)  7.7 us
    all_to_all x1, waiting for transfers between devices, body(): got = lax.all_to_all(sent, ('z', 'x'), 0, 0, tiled=True)  7.43 us
    all_to_all x1, starting transfers between devices, spread_rows(): return lax.all_to_all(copies, ('z', 'x'), 0, 0, tiled=True)  7.28 us
    all_to_all x1, waiting for transfers between devices, spread_rows(): return lax.all_to_all(copies, ('z', 'x'), 0, 0, tiled=True)  5.54 us
  transfers between devices with their start and end apart: 27, of which 11 were waited for; matrix products, arithmetic and copies ran while one was open for 2% of the time, Pallas kernels for 10%

profile of v3, /device:TPU:0, one launch (start us, length us, event | category | flops | bytes accessed | tf_op | source)
XLA Modules:
  0.0 99.6 jit_solution(17705203880962247372)
XLA Ops:
  1.5 7.3 %all-to-all-start = ((bf16[8,16,1024]{2,1,0:T(8,128)(2,1)}), bf16[8,16,1024]{2,1,0:T(8,128)(2,1)S(1)}, u32[]{:S(2)}, u32[]{:S(2)}) async-start(bf16[8,16,1024]{2,1,0:T(8,128)(2,1)} %broadcast_in_dim.28), calls=%async_computation | async-start | bytes 524288 | tf_op jit(solution)/shard_map/all_to_all | solution.py:45
  9.9 1.6 %shard_map.199 = (f32[1,1024]{1,0:T(1,128)S(1)}, f32[1,2048]{1,0:T(1,128)S(1)}, bf16[16,16,4096]{2,1,0:T(8,128)(2,1)S(1)}) custom-call(f32[1,1024]{1,0:T(1,128)} %bitcast.22, f32[1,2048]{1,0:T(1,128)} %bitcast.21, bf16[16,16,4096]{2,1,0:T(8,128)(2,1)} %refs_2_.2), custom_call_target="tpu_custom_call" | custom-call | tf_op jit(solution)/shard_map/pallas_call | solution.py:112
  12.1 5.5 %all-to-all-done.refs_0_ = bf16[8,16,1024]{2,1,0:T(8,128)(2,1)S(1)} async-done(((bf16[8,16,1024]{2,1,0:T(8,128)(2,1)}), bf16[8,16,1024]{2,1,0:T(8,128)(2,1)S(1)}, u32[]{:S(2)}, u32[]{:S(2)}) %all-to-all-start) | async-done | bytes 262176 | tf_op jit(solution)/shard_map/all_to_all | solution.py:45
  17.7 3.8 %shard_map.200 = bf16[8,5,2,16,128]{4,3,2,1,0:T(8,128)(2,1)} custom-call(s32[5]{0:T(128)S(1)} %stack.19.place, bf16[8,16,1024]{2,1,0:T(8,128)(2,1)S(1)} %all-to-all-done.refs_0_, f32[1,1024]{1,0:T(1,128)S(1)} %get-tuple-element.13.refs_1_, bf16[1024,128]{1,0:T(8,128)(2,1)S(1)} %collective-permute-done.refs_2_, ...), custom_call_target="tpu_custom_call" | custom-call | tf_op jit(solution)/shard_map/pallas_call | solution.py:84
  21.6 3.6 %all-to-all-start.1 = ((bf16[8,5,2,16,128]{4,3,2,1,0:T(8,128)(2,1)}), bf16[8,5,2,16,128]{4,3,2,1,0:T(8,128)(2,1)S(1)}, u32[]{:S(2)}, u32[]{:S(2)}) async-start(bf16[8,5,2,16,128]{4,3,2,1,0:T(8,128)(2,1)} %shard_map.200), calls=%async_computation.1 | async-start | bytes 655360 | tf_op jit(solution)/shard_map/all_to_all | solution.py:585
  25.1 2.0 %collective-permute-start.10 = (bf16[1024,128]{1,0:T(8,128)(2,1)}, bf16[1024,128]{1,0:T(8,128)(2,1)S(1)}, u32[]{:S(2)}, u32[]{:S(2)}) collective-permute-start(bf16[1024,128]{1,0:T(8,128)(2,1)} %refs_8_.3), channel_id=1, source_target_pairs={{0,4},{4,0},{1,5},{5,1},{2,6},{6,2},{3,7},{7,3},{8,12},{12,8},{9,1... | collective-permute-start | bytes 786440 | tf_op jit(solution)/shard_map/ppermute | solution.py:35
  27.7 7.4 %all-to-all-done.1.refs_0_ = bf16[8,5,2,16,128]{4,3,2,1,0:T(8,128)(2,1)S(1)} async-done(((bf16[8,5,2,16,128]{4,3,2,1,0:T(8,128)(2,1)}), bf16[8,5,2,16,128]{4,3,2,1,0:T(8,128)(2,1)S(1)}, u32[]{:S(2)}, u32[]{:S(2)}) %all-to-all-start.1) | async-done | bytes 327712 | tf_op jit(solution)/shard_map/all_to_all | solution.py:585
  38.0 3.3 %collective-permute-done.5.refs_3_ = bf16[42,16,128]{2,1,0:T(8,128)(2,1)} collective-permute-done((bf16[42,16,128]{2,1,0:T(8,128)(2,1)S(1)}, bf16[42,16,128]{2,1,0:T(8,128)(2,1)}, u32[]{:S(2)}, u32[]{:S(2)}) %collective-permute-start.5) | collective-permute-done | bytes 172064 | tf_op jit(solution)/shard_map/ppermute | solution.py:35
  41.3 4.2 %shard_map.202.refs_1_ = bf16[16,1024]{1,0:T(8,128)(2,1)S(1)} custom-call(s32[5]{0:T(128)S(1)} %stack.19.place, bf16[8,5,2,16,128]{4,3,2,1,0:T(8,128)(2,1)S(1)} %all-to-all-done.1.refs_0_, bf16[16,1024]{1,0:T(8,128)(2,1)S(1)} %copy-done.6, bf16[16,16,4096]{2,1,0:T(8,128)(2,1)S(1)} %get-tuple-element.14.refs_2_, ...), custom_call_target="tpu_custom_call" | custom-call | tf_op jit(solution)/shard_map/pallas_call | solution.py:84
  47.4 2.0 %collective-permute-done.6.refs_2_ = bf16[16,1024]{1,0:T(8,128)(2,1)S(1)} collective-permute-done((bf16[16,1024]{1,0:T(8,128)(2,1)S(1)}, bf16[16,1024]{1,0:T(8,128)(2,1)S(1)}, u32[]{:S(2)}, u32[]{:S(2)}) %collective-permute-start.6) | collective-permute-done | bytes 32800 | tf_op jit(solution)/shard_map/ppermute | solution.py:35
  51.6 3.6 %collective-permute-done.8.refs_4_ = bf16[16,1024]{1,0:T(8,128)(2,1)S(1)} collective-permute-done((bf16[16,1024]{1,0:T(8,128)(2,1)S(1)}, bf16[16,1024]{1,0:T(8,128)(2,1)S(1)}, u32[]{:S(2)}, u32[]{:S(2)}) %collective-permute-start.8) | collective-permute-done | bytes 32800 | tf_op jit(solution)/shard_map/ppermute | solution.py:35
  55.2 1.8 %shard_map.203.refs_1_ = bf16[4,4,16,128]{3,2,1,0:T(8,128)(2,1)S(1)} custom-call(s32[5]{0:T(128)S(1)} %stack.19.place, bf16[8,16,1024]{2,1,0:T(8,128)(2,1)S(1)} %all-to-all-done.refs_0_, bf16[16,1024]{1,0:T(8,128)(2,1)S(1)} %shard_map.202.refs_1_, bf16[16,1024]{1,0:T(8,128)(2,1)S(1)} %collective-permute-done.6.refs_2_, ...), custom_call_target="tpu_custom_call" | custom-call | tf_op jit(solution)/shard_map/pallas_call | solution.py:84
  57.0 1.6 %collective-permute-start.12 = (bf16[4,4,16,128]{3,2,1,0:T(8,128)(2,1)S(1)}, bf16[4,4,16,128]{3,2,1,0:T(8,128)(2,1)S(1)}, u32[]{:S(2)}, u32[]{:S(2)}) collective-permute-start(bf16[4,4,16,128]{3,2,1,0:T(8,128)(2,1)S(1)} %shard_map.203.refs_1_), channel_id=1, source_target_pairs={{0,1},{1,0},{2,3},{3,2},{4,5},{5,4},{6,7},{7,6},{8,9},{9,8},{10,11... | collective-permute-start | bytes 196616 | tf_op jit(solution)/shard_map/ppermute | solution.py:35
  58.7 2.7 %collective-permute-done.12.refs_2_ = bf16[4,4,16,128]{3,2,1,0:T(8,128)(2,1)S(1)} collective-permute-done((bf16[4,4,16,128]{3,2,1,0:T(8,128)(2,1)S(1)}, bf16[4,4,16,128]{3,2,1,0:T(8,128)(2,1)S(1)}, u32[]{:S(2)}, u32[]{:S(2)}) %collective-permute-start.12) | collective-permute-done | bytes 65568 | tf_op jit(solution)/shard_map/ppermute | solution.py:35
  63.4 2.1 %collective-permute-start.15 = (bf16[17,16,128]{2,1,0:T(8,128)(2,1)S(1)}, bf16[17,16,128]{2,1,0:T(8,128)(2,1)S(1)}, u32[]{:S(2)}, u32[]{:S(2)}) collective-permute-start(bf16[17,16,128]{2,1,0:T(8,128)(2,1)S(1)} %shard_map.204.refs_0_), channel_id=1, source_target_pairs={{0,12},{4,8},{8,4},{12,0},{16,28},{20,24},{24,20},{28,16},{1,13},{... | collective-permute-start | bytes 208904 | tf_op jit(solution)/shard_map/ppermute | solution.py:40
  65.8 3.5 %collective-permute-start.17 = (bf16[17,16,128]{2,1,0:T(8,128)(2,1)S(1)}, bf16[17,16,128]{2,1,0:T(8,128)(2,1)S(1)}, u32[]{:S(2)}, u32[]{:S(2)}) collective-permute-start(bf16[17,16,128]{2,1,0:T(8,128)(2,1)S(1)} %shard_map.204.refs_0_), channel_id=1, source_target_pairs={{0,20},{4,16},{8,28},{12,24},{16,4},{20,0},{24,12},{28,8},{1,21},{... | collective-permute-start | bytes 208904 | tf_op jit(solution)/shard_map/ppermute | solution.py:40
  69.3 1.7 %collective-permute-start.18 = (bf16[17,16,128]{2,1,0:T(8,128)(2,1)S(1)}, bf16[17,16,128]{2,1,0:T(8,128)(2,1)S(1)}, u32[]{:S(2)}, u32[]{:S(2)}) collective-permute-start(bf16[17,16,128]{2,1,0:T(8,128)(2,1)S(1)} %shard_map.204.refs_0_), channel_id=1, source_target_pairs={{0,24},{4,28},{8,16},{12,20},{16,8},{20,12},{24,0},{28,4},{1,25},{... | collective-permute-start | bytes 208904 | tf_op jit(solution)/shard_map/ppermute | solution.py:40
  71.0 2.1 %collective-permute-start.19 = (bf16[17,16,128]{2,1,0:T(8,128)(2,1)S(1)}, bf16[17,16,128]{2,1,0:T(8,128)(2,1)S(1)}, u32[]{:S(2)}, u32[]{:S(2)}) collective-permute-start(bf16[17,16,128]{2,1,0:T(8,128)(2,1)S(1)} %shard_map.204.refs_0_), channel_id=1, source_target_pairs={{0,28},{4,24},{8,20},{12,16},{16,12},{20,8},{24,4},{28,0},{1,29},{... | collective-permute-start | bytes 208904 | tf_op jit(solution)/shard_map/ppermute | solution.py:40
  73.1 2.4 %collective-permute-done.17.refs_5_ = bf16[17,16,128]{2,1,0:T(8,128)(2,1)S(1)} collective-permute-done((bf16[17,16,128]{2,1,0:T(8,128)(2,1)S(1)}, bf16[17,16,128]{2,1,0:T(8,128)(2,1)S(1)}, u32[]{:S(2)}, u32[]{:S(2)}) %collective-permute-start.17) | collective-permute-done | bytes 69664 | tf_op jit(solution)/shard_map/ppermute | solution.py:40
  75.6 2.4 %collective-permute-done.19.refs_7_ = bf16[17,16,128]{2,1,0:T(8,128)(2,1)S(1)} collective-permute-done((bf16[17,16,128]{2,1,0:T(8,128)(2,1)S(1)}, bf16[17,16,128]{2,1,0:T(8,128)(2,1)S(1)}, u32[]{:S(2)}, u32[]{:S(2)}) %collective-permute-start.19) | collective-permute-done | bytes 69664 | tf_op jit(solution)/shard_map/ppermute | solution.py:40
  78.0 3.6 %shard_map.205 = (bf16[8,2,16,1024]{3,2,1,0:T(8,128)(2,1)S(1)}, bf16[16,1024]{1,0:T(8,128)(2,1)S(1)}, bf16[16,2048]{1,0:T(8,128)(2,1)S(1)}) custom-call(s32[5]{0:T(128)S(1)} %stack.19.place, bf16[17,16,128]{2,1,0:T(8,128)(2,1)S(1)} %shard_map.204.refs_0_, bf16[17,16,128]{2,1,0:T(8,128)(2,1)S(1)} %collective-permute-done.13.refs_1_, ...), custom_call_target="tpu_custom_call" | custom-call | tf_op jit(solution)/shard_map/pallas_call | solution.py:84
  82.5 4.5 %all-to-all-start.2 = ((bf16[16,16,1024]{2,1,0:T(8,128)(2,1)}), bf16[16,16,1024]{2,1,0:T(8,128)(2,1)}, u32[]{:S(2)}, u32[]{:S(2)}) async-start(bf16[16,16,1024]{2,1,0:T(8,128)(2,1)} %bitcast.18), calls=%async_computation.2 | async-start | bytes 1048576 | tf_op jit(solution)/shard_map/all_to_all | solution.py:619
  88.2 1.9 %collective-permute-start.23 = (bf16[16,1024]{1,0:T(8,128)(2,1)S(1)}, bf16[16,1024]{1,0:T(8,128)(2,1)S(1)}, u32[]{:S(2)}, u32[]{:S(2)}) collective-permute-start(bf16[16,1024]{1,0:T(8,128)(2,1)S(1)} %get-tuple-element.19), channel_id=1, source_target_pairs={{0,1},{1,0},{2,3},{3,2},{4,5},{5,4},{6,7},{7,6},{8,9},{9,8},{10,11... | collective-permute-start | bytes 98312 | tf_op jit(solution)/shard_map/ppermute | solution.py:35
  90.2 7.7 %all-to-all-done.2 = bf16[16,16,1024]{2,1,0:T(8,128)(2,1)} async-done(((bf16[16,16,1024]{2,1,0:T(8,128)(2,1)}), bf16[16,16,1024]{2,1,0:T(8,128)(2,1)}, u32[]{:S(2)}, u32[]{:S(2)}) %all-to-all-start.2) | async-done | bytes 524320 | tf_op jit(solution)/shard_map/all_to_all | solution.py:619
  (70 shorter events, 16.8 us)
Async XLA Ops:
  1.5 16.2 %all-to-all-start = ((bf16[8,16,1024]{2,1,0:T(8,128)(2,1)}), bf16[8,16,1024]{2,1,0:T(8,128)(2,1)S(1)}, u32[]{:S(2)}, u32[]{:S(2)}) async-start(bf16[8,16,1024]{2,1,0:T(8,128)(2,1)} %broadcast_in_dim.28), calls=%async_computation | async-start | bytes 524288 | tf_op jit(solution)/shard_map/all_to_all | solution.py:45
  8.8 2.9 %collective-permute-start = (bf16[1024,128]{1,0:T(8,128)(2,1)}, bf16[1024,128]{1,0:T(8,128)(2,1)S(1)}, u32[]{:S(2)}, u32[]{:S(2)}) collective-permute-start(bf16[1024,128]{1,0:T(8,128)(2,1)} %refs_7_.1), channel_id=1, source_target_pairs={{0,2},{2,0},{1,3},{3,1},{4,6},{6,4},{5,7},{7,5},{8,10},{10,8},{9,1... | collective-permute-start | bytes 786440 | tf_op jit(solution)/shard_map/ppermute | solution.py:35
  8.8 2.9 %collective-permute-start.1 = (bf16[1024,128]{1,0:T(8,128)(2,1)}, bf16[1024,128]{1,0:T(8,128)(2,1)S(1)}, u32[]{:S(2)}, u32[]{:S(2)}) collective-permute-start(bf16[1024,128]{1,0:T(8,128)(2,1)} %refs_8_.2), channel_id=1, source_target_pairs={{0,2},{2,0},{1,3},{3,1},{4,6},{6,4},{5,7},{7,5},{8,10},{10,8},{9,1... | collective-permute-start | bytes 786440 | tf_op jit(solution)/shard_map/ppermute | solution.py:35
  21.6 13.6 %all-to-all-start.1 = ((bf16[8,5,2,16,128]{4,3,2,1,0:T(8,128)(2,1)}), bf16[8,5,2,16,128]{4,3,2,1,0:T(8,128)(2,1)S(1)}, u32[]{:S(2)}, u32[]{:S(2)}) async-start(bf16[8,5,2,16,128]{4,3,2,1,0:T(8,128)(2,1)} %shard_map.200), calls=%async_computation.1 | async-start | bytes 655360 | tf_op jit(solution)/shard_map/all_to_all | solution.py:585
  25.1 12.1 %collective-permute-start.10 = (bf16[1024,128]{1,0:T(8,128)(2,1)}, bf16[1024,128]{1,0:T(8,128)(2,1)S(1)}, u32[]{:S(2)}, u32[]{:S(2)}) collective-permute-start(bf16[1024,128]{1,0:T(8,128)(2,1)} %refs_8_.3), channel_id=1, source_target_pairs={{0,4},{4,0},{1,5},{5,1},{2,6},{6,2},{3,7},{7,3},{8,12},{12,8},{9,1... | collective-permute-start | bytes 786440 | tf_op jit(solution)/shard_map/ppermute | solution.py:35
  27.2 36.2 %collective-permute-start.20 = (bf16[2048,256]{1,0:T(8,128)(2,1)}, bf16[2048,256]{1,0:T(8,128)(2,1)}, u32[]{:S(2)}, u32[]{:S(2)}) collective-permute-start(bf16[2048,256]{1,0:T(8,128)(2,1)} %bitcast.14), channel_id=1, source_target_pairs={{0,2},{2,0},{1,3},{3,1},{4,6},{6,4},{5,7},{7,5},{8,10},{10,8},{9,1... | collective-permute-start | bytes 3145736 | tf_op jit(solution)/shard_map/ppermute | solution.py:35
  27.2 38.3 %collective-permute-start.21 = (bf16[2048,256]{1,0:T(8,128)(2,1)}, bf16[2048,256]{1,0:T(8,128)(2,1)}, u32[]{:S(2)}, u32[]{:S(2)}) collective-permute-start(bf16[2048,256]{1,0:T(8,128)(2,1)} %bitcast.16), channel_id=1, source_target_pairs={{0,2},{2,0},{1,3},{3,1},{4,6},{6,4},{5,7},{7,5},{8,10},{10,8},{9,1... | collective-permute-start | bytes 3145736 | tf_op jit(solution)/shard_map/ppermute | solution.py:35
  27.7 38.1 %collective-permute-start.22 = (bf16[256,2048]{1,0:T(8,128)(2,1)}, bf16[256,2048]{1,0:T(8,128)(2,1)}, u32[]{:S(2)}, u32[]{:S(2)}) collective-permute-start(bf16[256,2048]{1,0:T(8,128)(2,1)} %bitcast.19), channel_id=1, source_target_pairs={{0,2},{2,0},{1,3},{3,1},{4,6},{6,4},{5,7},{7,5},{8,10},{10,8},{9,1... | collective-permute-start | bytes 3145736 | tf_op jit(solution)/shard_map/ppermute | solution.py:35
  35.7 5.5 %collective-permute-start.5 = (bf16[42,16,128]{2,1,0:T(8,128)(2,1)S(1)}, bf16[42,16,128]{2,1,0:T(8,128)(2,1)}, u32[]{:S(2)}, u32[]{:S(2)}) collective-permute-start(bf16[42,16,128]{2,1,0:T(8,128)(2,1)S(1)} %shard_map.201), channel_id=1, source_target_pairs={{0,1},{1,0},{2,3},{3,2},{4,5},{5,4},{6,7},{7,6},{8,9},{9,8},{10,11... | collective-permute-start | bytes 516104 | tf_op jit(solution)/shard_map/ppermute | solution.py:35
  37.3 8.2 %collective-permute-start.9 = (bf16[1024,128]{1,0:T(8,128)(2,1)}, bf16[1024,128]{1,0:T(8,128)(2,1)S(1)}, u32[]{:S(2)}, u32[]{:S(2)}) collective-permute-start(bf16[1024,128]{1,0:T(8,128)(2,1)} %refs_8_.3), channel_id=1, source_target_pairs={{0,2},{2,0},{1,3},{3,1},{4,6},{6,4},{5,7},{7,5},{8,10},{10,8},{9,1... | collective-permute-start | bytes 786440 | tf_op jit(solution)/shard_map/ppermute | solution.py:35
  41.3 5.5 %collective-permute-start.11 = (bf16[1024,128]{1,0:T(8,128)(2,1)S(1)}, bf16[1024,128]{1,0:T(8,128)(2,1)S(1)}, u32[]{:S(2)}, u32[]{:S(2)}) collective-permute-start(bf16[1024,128]{1,0:T(8,128)(2,1)S(1)} %collective-permute-done.10.refs_6_), channel_id=1, source_target_pairs={{0,2},{2,0},{1,3},{3,1},{4,6},{6,4},{5,7},{7,5},{8,10},{10,8},{9,1... | collective-permute-start | bytes 786440 | tf_op jit(solution)/shard_map/ppermute | solution.py:35
  45.5 4.0 %collective-permute-start.6 = (bf16[16,1024]{1,0:T(8,128)(2,1)S(1)}, bf16[16,1024]{1,0:T(8,128)(2,1)S(1)}, u32[]{:S(2)}, u32[]{:S(2)}) collective-permute-start(bf16[16,1024]{1,0:T(8,128)(2,1)S(1)} %shard_map.202.refs_1_), channel_id=1, source_target_pairs={{0,8},{8,0},{16,24},{24,16},{1,9},{9,1},{17,25},{25,17},{2,10},{10... | collective-permute-start | bytes 98312 | tf_op jit(solution)/shard_map/ppermute | solution.py:35
  46.8 4.9 %collective-permute-start.7 = (bf16[16,1024]{1,0:T(8,128)(2,1)S(1)}, bf16[16,1024]{1,0:T(8,128)(2,1)S(1)}, u32[]{:S(2)}, u32[]{:S(2)}) collective-permute-start(bf16[16,1024]{1,0:T(8,128)(2,1)S(1)} %shard_map.202.refs_1_), channel_id=1, source_target_pairs={{0,16},{8,24},{16,0},{24,8},{1,17},{9,25},{17,1},{25,9},{2,18},{10... | collective-permute-start | bytes 98312 | tf_op jit(solution)/shard_map/ppermute | solution.py:35
  49.5 5.7 %collective-permute-start.8 = (bf16[16,1024]{1,0:T(8,128)(2,1)S(1)}, bf16[16,1024]{1,0:T(8,128)(2,1)S(1)}, u32[]{:S(2)}, u32[]{:S(2)}) collective-permute-start(bf16[16,1024]{1,0:T(8,128)(2,1)S(1)} %shard_map.202.refs_1_), channel_id=1, source_target_pairs={{0,24},{8,16},{16,8},{24,0},{1,25},{9,17},{17,9},{25,1},{2,26},{10... | collective-permute-start | bytes 98312 | tf_op jit(solution)/shard_map/ppermute | solution.py:35
  57.0 4.3 %collective-permute-start.12 = (bf16[4,4,16,128]{3,2,1,0:T(8,128)(2,1)S(1)}, bf16[4,4,16,128]{3,2,1,0:T(8,128)(2,1)S(1)}, u32[]{:S(2)}, u32[]{:S(2)}) collective-permute-start(bf16[4,4,16,128]{3,2,1,0:T(8,128)(2,1)S(1)} %shard_map.203.refs_1_), channel_id=1, source_target_pairs={{0,1},{1,0},{2,3},{3,2},{4,5},{5,4},{6,7},{7,6},{8,9},{9,8},{10,11... | collective-permute-start | bytes 196616 | tf_op jit(solution)/shard_map/ppermute | solution.py:35
  61.9 7.4 %collective-permute-start.13 = (bf16[17,16,128]{2,1,0:T(8,128)(2,1)S(1)}, bf16[17,16,128]{2,1,0:T(8,128)(2,1)S(1)}, u32[]{:S(2)}, u32[]{:S(2)}) collective-permute-start(bf16[17,16,128]{2,1,0:T(8,128)(2,1)S(1)} %shard_map.204.refs_0_), channel_id=1, source_target_pairs={{0,4},{4,0},{8,12},{12,8},{16,20},{20,16},{24,28},{28,24},{1,5},{5... | collective-permute-start | bytes 208904 | tf_op jit(solution)/shard_map/ppermute | solution.py:40
  63.4 7.6 %collective-permute-start.14 = (bf16[17,16,128]{2,1,0:T(8,128)(2,1)S(1)}, bf16[17,16,128]{2,1,0:T(8,128)(2,1)S(1)}, u32[]{:S(2)}, u32[]{:S(2)}) collective-permute-start(bf16[17,16,128]{2,1,0:T(8,128)(2,1)S(1)} %shard_map.204.refs_0_), channel_id=1, source_target_pairs={{0,8},{4,12},{8,0},{12,4},{16,24},{20,28},{24,16},{28,20},{1,9},{5... | collective-permute-start | bytes 208904 | tf_op jit(solution)/shard_map/ppermute | solution.py:40
  63.4 9.7 %collective-permute-start.15 = (bf16[17,16,128]{2,1,0:T(8,128)(2,1)S(1)}, bf16[17,16,128]{2,1,0:T(8,128)(2,1)S(1)}, u32[]{:S(2)}, u32[]{:S(2)}) collective-permute-start(bf16[17,16,128]{2,1,0:T(8,128)(2,1)S(1)} %shard_map.204.refs_0_), channel_id=1, source_target_pairs={{0,12},{4,8},{8,4},{12,0},{16,28},{20,24},{24,20},{28,16},{1,13},{... | collective-permute-start | bytes 208904 | tf_op jit(solution)/shard_map/ppermute | solution.py:40
  65.5 7.7 %collective-permute-start.16 = (bf16[17,16,128]{2,1,0:T(8,128)(2,1)S(1)}, bf16[17,16,128]{2,1,0:T(8,128)(2,1)S(1)}, u32[]{:S(2)}, u32[]{:S(2)}) collective-permute-start(bf16[17,16,128]{2,1,0:T(8,128)(2,1)S(1)} %shard_map.204.refs_0_), channel_id=1, source_target_pairs={{0,16},{4,20},{8,24},{12,28},{16,0},{20,4},{24,8},{28,12},{1,17},{... | collective-permute-start | bytes 208904 | tf_op jit(solution)/shard_map/ppermute | solution.py:40
  65.8 9.8 %collective-permute-start.17 = (bf16[17,16,128]{2,1,0:T(8,128)(2,1)S(1)}, bf16[17,16,128]{2,1,0:T(8,128)(2,1)S(1)}, u32[]{:S(2)}, u32[]{:S(2)}) collective-permute-start(bf16[17,16,128]{2,1,0:T(8,128)(2,1)S(1)} %shard_map.204.refs_0_), channel_id=1, source_target_pairs={{0,20},{4,16},{8,28},{12,24},{16,4},{20,0},{24,12},{28,8},{1,21},{... | collective-permute-start | bytes 208904 | tf_op jit(solution)/shard_map/ppermute | solution.py:40
  69.3 6.3 %collective-permute-start.18 = (bf16[17,16,128]{2,1,0:T(8,128)(2,1)S(1)}, bf16[17,16,128]{2,1,0:T(8,128)(2,1)S(1)}, u32[]{:S(2)}, u32[]{:S(2)}) collective-permute-start(bf16[17,16,128]{2,1,0:T(8,128)(2,1)S(1)} %shard_map.204.refs_0_), channel_id=1, source_target_pairs={{0,24},{4,28},{8,16},{12,20},{16,8},{20,12},{24,0},{28,4},{1,25},{... | collective-permute-start | bytes 208904 | tf_op jit(solution)/shard_map/ppermute | solution.py:40
  71.0 7.0 %collective-permute-start.19 = (bf16[17,16,128]{2,1,0:T(8,128)(2,1)S(1)}, bf16[17,16,128]{2,1,0:T(8,128)(2,1)S(1)}, u32[]{:S(2)}, u32[]{:S(2)}) collective-permute-start(bf16[17,16,128]{2,1,0:T(8,128)(2,1)S(1)} %shard_map.204.refs_0_), channel_id=1, source_target_pairs={{0,28},{4,24},{8,20},{12,16},{16,12},{20,8},{24,4},{28,0},{1,29},{... | collective-permute-start | bytes 208904 | tf_op jit(solution)/shard_map/ppermute | solution.py:40
  82.5 15.4 %all-to-all-start.2 = ((bf16[16,16,1024]{2,1,0:T(8,128)(2,1)}), bf16[16,16,1024]{2,1,0:T(8,128)(2,1)}, u32[]{:S(2)}, u32[]{:S(2)}) async-start(bf16[16,16,1024]{2,1,0:T(8,128)(2,1)} %bitcast.18), calls=%async_computation.2 | async-start | bytes 1048576 | tf_op jit(solution)/shard_map/all_to_all | solution.py:619
  88.2 10.8 %collective-permute-start.23 = (bf16[16,1024]{1,0:T(8,128)(2,1)S(1)}, bf16[16,1024]{1,0:T(8,128)(2,1)S(1)}, u32[]{:S(2)}, u32[]{:S(2)}) collective-permute-start(bf16[16,1024]{1,0:T(8,128)(2,1)S(1)} %get-tuple-element.19), channel_id=1, source_target_pairs={{0,1},{1,0},{2,3},{3,2},{4,5},{5,4},{6,7},{7,6},{8,9},{9,8},{10,11... | collective-permute-start | bytes 98312 | tf_op jit(solution)/shard_map/ppermute | solution.py:35
  (13 other events, 196.9 us)
